TPU v7x, 512 devices: a whole 4x8x8 slice. The times are simulated.
512 devices in a mesh: dp: 4 (over x), kv: 64 (over z, y), tp: 2 (over core).
Axes of the slice: x: 4, y: 8, z: 8, core: 2. Of those that a mesh axis runs over, the one named last changes fastest.
Arguments:
- token_state: bfloat16 [64, 4096], P('dp', 'kv'), may hold values from -150 to 150
- norm_gain: float32 [4096], P('kv'), may hold values from 0.1 to 1.9
- wq_nope: bfloat16 [4096, 1024], P('kv', 'tp'), may hold values from -0.09375 to 0.09375
- wq_rope: bfloat16 [4096, 512], P('kv', 'tp'), may hold values from -0.09375 to 0.09375
- w_latent: bfloat16 [4096, 512], P('kv'), may hold values from -0.09375 to 0.09375
- w_rope_key: bfloat16 [4096, 32], P('kv'), may hold values from -0.09375 to 0.09375
- kv_gain: float32 [512], replicated, may hold values from 0.1 to 1.9
- w_uk: bfloat16 [512, 1024], P('kv', 'tp'), may hold values from -0.25 to 0.25
- w_uv: bfloat16 [512, 1024], P('kv', 'tp'), may hold values from -6 to 6
- w_out: bfloat16 [1024, 4096], P('tp', 'kv'), may hold values from -0.1875 to 0.1875
- latent_cache: bfloat16 [64, 12288, 512], P('dp', 'kv'), may hold values from -500 to 500
- rope_cache: bfloat16 [64, 32, 12288], P('dp', None, 'kv'), may hold values from -6 to 6
- lengths: int32 [64], P('dp'), may hold values from 3072 to 12287, as said below
Outputs:
- mixed: bfloat16 [64, 4096], P('dp', ('kv', 'tp'))
- latent_new: bfloat16 [64, 512], P('dp')
- rope_new: bfloat16 [64, 32], P('dp')
Inputs may be any that keep to these rules, and one draw needn't show every extreme that they name: Sequence b has cached positions 0 to lengths[b] - 1 and its new token takes position lengths[b]; in each aligned block of 16 sequences one has length 12287.
All inputs are finite; a program needn't handle non-finite values.
Results may differ from a plain program's by a relative error of at most 0.02.
Values may be sent and summed in bfloat16 or wider, within the bound.
No kernel may reach another device: no remote copies, remote signals or barrier semaphores. Data moves between devices by JAX's collectives and lax.ppermute only.
A program may use at most 64 MiB of HBM per device.

v0:
```python
import functools

import jax
import jax.numpy as jnp
from jax import lax
from jax.sharding import Mesh
from jax.sharding import PartitionSpec as P

D = 4096
NOPE = 64
ROPE = 32
V_DIM = 64
KV = ("kv_0", "kv_1")
KV_TP = ("kv_0", "kv_1", "tp")


EPS = 1e-06
THETA = 10000.0
NEG = -1e30


def padded_to(lines, devices):
    spare = -lines.shape[0] % devices
    if not spare:
        return lines
    return jnp.concatenate([lines, jnp.zeros((spare, *lines.shape[1:]), lines.dtype)])


def in_order(parts, dim):
    parts = jnp.moveaxis(parts, 0, dim)
    lengths = parts.shape
    return parts.reshape(*lengths[:dim], lengths[dim] * lengths[dim + 1], *lengths[dim + 2 :])


def sent_to_all(value, axis):
    devices = lax.axis_size(axis)
    return lax.all_to_all(
        jnp.broadcast_to(value[None], (devices, *value.shape)), axis, 0, 0, tiled=True
    )


def gather_directly(value, axis, dim):
    return in_order(sent_to_all(value, axis), dim)


def in_blocks(value, dim, devices):
    lengths = value.shape
    parts = value.reshape(*lengths[:dim], devices, lengths[dim] // devices, *lengths[dim + 1 :])
    return jnp.moveaxis(parts, dim, 0)


def sent_and_summed(value, axis, dim):
    parts = in_blocks(value, dim, lax.axis_size(axis))
    arrived = lax.all_to_all(parts, axis, split_axis=0, concat_axis=0, tiled=True)
    return arrived.sum(axis=0)


def nested_sum(value, axes):
    padded = padded_to(value, lax.axis_size(axes))
    whole = gather_directly(sent_and_summed(padded, axes, 0), axes, 0)
    return lax.slice_in_dim(whole, 0, len(value)).reshape(value.shape)


def packed_total(arrays, axis):
    ends = [0]
    for a in arrays:
        ends.append(ends[-1] + a.size)
    subtotal = nested_sum(jnp.concatenate([a.ravel() for a in arrays]), axis)
    return tuple((subtotal[b:e].reshape(a.shape) for a, b, e in zip(arrays, ends, ends[1:])))


def over_axes(value, axes):
    return functools.reduce(lax.pmax, axes, value)


def summed_rows(value, axes, dim):
    far, near = axes
    own = sent_and_summed(in_blocks(value, dim, lax.axis_size(far)), near, dim + 1)
    return jnp.sum(lax.all_to_all(own, far, 0, 0, tiled=True), axis=0)


def summed_on_arrival(value, axis, dim):
    parts = in_blocks(value, dim, lax.axis_size(axis))
    arrived = lax.all_to_all(parts, axis, split_axis=0, concat_axis=0, tiled=True)
    return arrived.astype(jnp.float32).sum(axis=0)


def rotate(vector, angles):
    half_dim = vector.shape[-1] // 2
    cosine = jnp.cos(angles)
    sine_part = jnp.sin(angles)
    leading = vector[..., :half_dim]
    trailing = vector[..., half_dim:]
    return jnp.concatenate(
        [leading * cosine - trailing * sine_part, trailing * cosine + leading * sine_part], axis=-1
    )


def rope_angles(lengths):
    half_dim = ROPE // 2
    inv_freq = THETA ** (-jnp.arange(half_dim, dtype=jnp.float32) * 2.0 / ROPE)
    return lengths.astype(jnp.float32)[:, None] * inv_freq[None, :]


def local(
    token_state,
    norm_gain,
    wq_nope,
    wq_rope,
    w_latent,
    w_rope_key,
    kv_gain,
    w_uk,
    w_uv,
    w_out,
    latent_cache,
    rope_cache,
    lengths,
):
    x_wide = token_state.astype(jnp.float32)
    scaled = (x_wide * norm_gain).astype(jnp.bfloat16)
    partials = (
        jnp.sum(x_wide * x_wide, axis=1),
        jnp.dot(scaled, wq_nope, preferred_element_type=jnp.float32),
        jnp.dot(scaled, wq_rope, preferred_element_type=jnp.float32),
        jnp.dot(scaled, w_latent, preferred_element_type=jnp.float32),
        jnp.dot(scaled, w_rope_key, preferred_element_type=jnp.float32),
    )
    squares, nope_sum, rope_sum, latent_sum, key_sum = packed_total(
        (partials[0], partials[1], partials[2], partials[3], partials[4]), KV
    )
    inv_rms = lax.rsqrt(squares / D + EPS)[:, None]
    seq_count = token_state.shape[0]
    head_count = wq_nope.shape[1] // NOPE
    latent_raw = latent_sum * inv_rms
    latent_new = (
        latent_raw
        * lax.rsqrt(jnp.mean(latent_raw * latent_raw, axis=1, keepdims=True) + EPS)
        * kv_gain
    ).astype(jnp.bfloat16)
    angles = rope_angles(lengths)
    rope_new = rotate(key_sum * inv_rms, angles).astype(jnp.bfloat16)
    q_rot = rotate(
        (rope_sum * inv_rms).reshape(seq_count, head_count, ROPE), angles[:, None, :]
    ).astype(jnp.bfloat16)
    q_low = (nope_sum * inv_rms).astype(jnp.bfloat16).reshape(seq_count, head_count, NOPE)
    row_count = w_uk.shape[0]
    q_piece = jnp.einsum(
        "bhn,rhn->bhr",
        q_low,
        w_uk.reshape(row_count, head_count, NOPE),
        preferred_element_type=jnp.float32,
    ).astype(jnp.bfloat16)
    q_latent = gather_directly(q_piece, KV, 2)
    block_len = latent_cache.shape[1]
    positions = lax.axis_index(KV) * block_len + jnp.arange(block_len, dtype=jnp.int32)
    score_scale = (NOPE + ROPE) ** (-0.5)
    cached = jnp.einsum("bhr,bpr->bhp", q_latent, latent_cache, preferred_element_type=jnp.float32)
    cached = cached + jnp.einsum(
        "bhk,bkp->bhp", q_rot, rope_cache, preferred_element_type=jnp.float32
    )
    own = jnp.einsum("bhr,br->bh", q_latent, latent_new, preferred_element_type=jnp.float32)
    own = own + jnp.einsum("bhk,bk->bh", q_rot, rope_new, preferred_element_type=jnp.float32)
    limit = lengths[:, None, None]
    newslot = positions[None, None, :] == limit
    usable = (positions[None, None, :] < limit) | newslot
    scores = jnp.where(newslot, own[:, :, None], cached) * score_scale
    masked = jnp.where(usable, scores, NEG)
    local_max = jnp.max(masked, axis=2)
    weights = jnp.where(usable, jnp.exp(masked - local_max[..., None]), 0.0)
    totals = jnp.sum(weights, axis=2)
    rounded = weights.astype(jnp.bfloat16)
    cache_weights = jnp.where(newslot, jnp.zeros_like(rounded), rounded)
    weighted = jnp.einsum(
        "bhp,bpr->bhr", cache_weights, latent_cache, preferred_element_type=jnp.float32
    )
    own_low = lax.optimization_barrier(jnp.where(newslot, rounded, jnp.zeros_like(rounded)))
    own_weight = jnp.sum(own_low.astype(jnp.float32), axis=2)
    weighted = weighted + own_weight[..., None] * latent_new.astype(jnp.float32)[:, None, :]
    value_rows = w_uv.shape[0]
    w_values = w_uv.reshape(value_rows, head_count, V_DIM)
    highest = over_axes(local_max, KV)
    factor = jnp.exp(local_max - highest)
    latent_piece = summed_rows(weighted * factor[..., None], ("kv_0", "kv_1"), 2).astype(
        jnp.bfloat16
    )
    partial_values = jnp.einsum(
        "bhr,rhv->bhv", latent_piece, w_values, preferred_element_type=jnp.float32
    )
    value_sum, totals = packed_total((partial_values, totals * factor), KV)
    values = value_sum / totals[:, :, None]
    attended = values.astype(jnp.bfloat16).reshape(seq_count, head_count * V_DIM)
    out_term = jnp.dot(attended, w_out, preferred_element_type=jnp.float32)
    mixed = summed_on_arrival(out_term.astype(jnp.bfloat16), "tp", 1).astype(jnp.bfloat16)
    return (mixed, latent_new, rope_new)


def solution(mesh):
    finer = Mesh(
        mesh.devices.reshape(mesh.shape["dp"], 8, 8, mesh.shape["tp"]), ("dp", "kv_0", "kv_1", "tp")
    )
    in_specs = (
        P("dp", KV),
        P(KV),
        P(KV, "tp"),
        P(KV, "tp"),
        P(KV, None),
        P(KV, None),
        P(),
        P(KV, "tp"),
        P(KV, "tp"),
        P("tp", KV),
        P("dp", KV, None),
        P("dp", None, KV),
        P("dp"),
    )
    out_specs = (P("dp", KV_TP), P("dp", None), P("dp", None))
    return jax.shard_map(local, mesh=finer, in_specs=in_specs, out_specs=out_specs, check_vma=False)
```

profile of v0, /device:TPU:1, one launch (start us, length us, event | category | flops | bytes accessed | tf_op | source)
XLA Modules:
  0.0 204.6 jit_solution(302552633651716855)
XLA Ops:
  0.6 1.0 fusion.16
  1.6 1.0 convolution_bitcast_fusion.2
  2.6 1.0 convolution_bitcast_fusion.1
  3.6 0.9 convolution_bitcast_fusion.3
  4.5 0.8 fusion.21
  5.6 0.9 all_to_all.32
  6.5 17.1 %all-to-all-start = ((f32[64,1,329]{2,1,0:T(1,128)}), f32[64,1,329]{2,1,0:T(1,128)S(1)}, u32[]{:S(2)}, u32[]{:S(2)}) async-start(f32[64,1,329]{2,1,0:T(1,128)} %all_to_all.32), calls=%async_computation | async-start | bytes 196608 | tf_op jit(solution)/shard_map/all_to_all | solution.py:54
  23.6 11.4 %all-to-all-done = f32[64,1,329]{2,1,0:T(1,128)S(1)} async-done(((f32[64,1,329]{2,1,0:T(1,128)}), f32[64,1,329]{2,1,0:T(1,128)S(1)}, u32[]{:S(2)}, u32[]{:S(2)}) %all-to-all-start) | async-done | bytes 84256 | tf_op jit(solution)/shard_map/all_to_all | solution.py:54
  35.1 0.7 broadcast_in_dim.82
  35.8 4.7 %all-to-all-start.1 = ((f32[64,1,329]{2,1,0:T(1,128)}), f32[64,1,329]{2,1,0:T(1,128)S(1)}, u32[]{:S(2)}, u32[]{:S(2)}) async-start(f32[64,1,329]{2,1,0:T(1,128)} %broadcast_in_dim.82), calls=%async_computation.1 | async-start | bytes 196608 | tf_op jit(solution)/shard_map/all_to_all | solution.py:37
  40.6 0.7 broadcast_compare_fusion
  41.3 0.7 convert_element_type.59
  42.0 0.8 reshape.295
  42.7 9.1 %all-to-all-done.1 = f32[64,1,329]{2,1,0:T(1,128)S(1)} async-done(((f32[64,1,329]{2,1,0:T(1,128)}), f32[64,1,329]{2,1,0:T(1,128)S(1)}, u32[]{:S(2)}, u32[]{:S(2)}) %all-to-all-start.1) | async-done | bytes 84256 | tf_op jit(solution)/shard_map/all_to_all | solution.py:37
  53.4 1.3 broadcast_bitcast_fusion
  54.6 3.1 %reshape.315 = bf16[64,2,512]{2,1,0:T(2,128)(2,1)} reshape(bf16[64,8,8,16]{3,2,1,0:T(8,128)(2,1)} %broadcast_bitcast_fusion) | data formatting | bytes 262144
  57.7 4.6 %all-to-all-start.2 = ((bf16[64,2,512]{2,1,0:T(2,128)(2,1)}), bf16[64,2,512]{2,1,0:T(2,128)(2,1)S(1)}, u32[]{:S(2)}, u32[]{:S(2)}) async-start(bf16[64,2,512]{2,1,0:T(2,128)(2,1)} %reshape.315), calls=%async_computation.2 | async-start | bytes 262144 | tf_op jit(solution)/shard_map/all_to_all | solution.py:37
  63.3 0.7 fusion.32
  64.0 9.9 %all-to-all-done.2 = bf16[64,2,512]{2,1,0:T(2,128)(2,1)S(1)} async-done(((bf16[64,2,512]{2,1,0:T(2,128)(2,1)}), bf16[64,2,512]{2,1,0:T(2,128)(2,1)S(1)}, u32[]{:S(2)}, u32[]{:S(2)}) %all-to-all-start.2) | async-done | bytes 131104 | tf_op jit(solution)/shard_map/all_to_all | solution.py:37
  73.9 1.7 reshape.316
  75.6 2.4 %copy_bitcast_fusion = bf16[16,8,512]{0,2,1:T(8,128)(2,1)} fusion(bf16[64,8,8,16]{3,2,1,0:T(8,128)(2,1)} %reshape.316), kind=kLoop, calls=%fused_computation.13 | loop fusion | bytes 262144 | tf_op jit(solution)/shard_map/reshape | solution.py:32
  78.0 1.6 copy.56
  79.6 0.9 fusion.9
  80.6 0.9 fusion.36
  81.8 11.6 %pmax.14 = f32[16,8]{1,0:T(8,128)S(1)} all-reduce(f32[16,8]{1,0:T(8,128)S(1)} %get-tuple-element.19), channel_id=1, replica_groups=mesh['dp'=4,'kv_0'=8,'kv_1'=8,'tp'=2] {'kv_0'}, use_global_device_ids=true, to_apply=%region_5.6 | all-reduce | flops 128 | bytes 1024 | tf_op jit(solution)/shard_map/pmax | solution.py:73
  93.8 0.7 convert_reduce_fusion
  94.5 11.4 %pmax.15 = f32[16,8]{1,0:T(8,128)S(1)} all-reduce(f32[16,8]{1,0:T(8,128)S(1)} %pmax.14), channel_id=1, replica_groups=mesh['dp'=4,'kv_0'=8,'kv_1'=8,'tp'=2] {'kv_1'}, use_global_device_ids=true, to_apply=%region_6.7 | all-reduce | flops 128 | bytes 1024 | tf_op jit(solution)/shard_map/pmax | solution.py:73
  106.5 1.3 fusion
  107.8 1.0 reshape.300
  108.7 3.0 %copy.57 = f32[16,8,8,64]{0,3,1,2:T(8,128)} copy(f32[16,8,8,64]{3,2,1,0:T(8,128)} %reshape.300) | data formatting | bytes 524288 | tf_op jit(solution)/shard_map/reshape | solution.py:48
  111.8 3.2 %copy_bitcast_fusion.2 = f32[8,8,8,8,16]{4,3,2,1,0:T(8,128)} fusion(f32[16,8,8,64]{0,3,1,2:T(8,128)} %copy.57), kind=kLoop, calls=%fused_computation.70 | loop fusion | bytes 524288
  114.9 2.4 %reshape.317 = f32[8,1,8192]{2,1,0:T(1,128)S(1)} reshape(f32[8,8,8,8,16]{4,3,2,1,0:T(8,128)} %copy_bitcast_fusion.2) | data formatting | bytes 524288
  117.3 13.1 %all_to_all.50 = f32[8,1,8192]{2,1,0:T(1,128)} all-to-all(f32[8,1,8192]{2,1,0:T(1,128)S(1)} %reshape.317), channel_id=1, replica_groups=mesh['dp'=4,'kv_0'=8,'kv_1'=8,'tp'=2] {'kv_1'}, dimensions={0} | all-to-all | bytes 524288 | tf_op jit(solution)/shard_map/all_to_all | solution.py:54
  130.9 2.2 %reduce.6 = f32[8,8192]{1,0:T(8,128)S(1)} reduce(f32[8,1,8192]{2,1,0:T(1,128)} %all_to_all.50, f32[]{:T(128)} %broadcast.183), dimensions={1}, to_apply=%all_to_all.36.reduce_sub_computation | reduce | bytes 524292 | tf_op jit(solution)/shard_map/all_to_all | solution.py:54
  133.2 2.1 %reshape.318 = f32[8,8,8,8,16]{4,3,2,1,0:T(8,128)} reshape(f32[8,8192]{1,0:T(8,128)S(1)} %reduce.6) | data formatting | bytes 524288
  135.2 1.8 bitcast_reduce_fusion
  137.1 0.8 reshape.319
  137.8 3.8 %all-to-all-start.4 = ((f32[8,1,1024]{2,1,0:T(1,128)}), f32[8,1,1024]{2,1,0:T(1,128)S(1)}, u32[]{:S(2)}, u32[]{:S(2)}) async-start(f32[8,1,1024]{2,1,0:T(1,128)} %reshape.319), calls=%async_computation.4 | async-start | bytes 65536 | tf_op jit(solution)/shard_map/all_to_all | solution.py:79
  141.8 6.7 %all-to-all-done.4 = f32[8,1,1024]{2,1,0:T(1,128)S(1)} async-done(((f32[8,1,1024]{2,1,0:T(1,128)}), f32[8,1,1024]{2,1,0:T(1,128)S(1)}, u32[]{:S(2)}, u32[]{:S(2)}) %all-to-all-start.4) | async-done | bytes 32800 | tf_op jit(solution)/shard_map/all_to_all | solution.py:79
  148.5 0.7 reduce.7
  149.9 14.9 %all_to_all.51 = f32[64,1,130]{2,1,0:T(1,128)S(1)} all-to-all(f32[64,1,130]{2,1,0:T(1,128)S(1)} %all_to_all.38), channel_id=1, replica_groups=mesh['dp'=4,'kv_0'=8,'kv_1'=8,'tp'=2] {'kv_0','kv_1'}, dimensions={0} | all-to-all | bytes 66560 | tf_op jit(solution)/shard_map/all_to_all | solution.py:54
  164.9 0.7 broadcast_in_dim.87
  165.5 4.6 %all-to-all-start.6 = ((f32[64,1,130]{2,1,0:T(1,128)}), f32[64,1,130]{2,1,0:T(1,128)S(1)}, u32[]{:S(2)}, u32[]{:S(2)}) async-start(f32[64,1,130]{2,1,0:T(1,128)} %broadcast_in_dim.87), calls=%async_computation.6 | async-start | bytes 131072 | tf_op jit(solution)/shard_map/all_to_all | solution.py:37
  170.2 0.7 pad_maximum_fusion.4
  170.8 10.4 %all-to-all-done.6 = f32[64,1,130]{2,1,0:T(1,128)S(1)} async-done(((f32[64,1,130]{2,1,0:T(1,128)}), f32[64,1,130]{2,1,0:T(1,128)S(1)}, u32[]{:S(2)}, u32[]{:S(2)}) %all-to-all-start.6) | async-done | bytes 33312 | tf_op jit(solution)/shard_map/all_to_all | solution.py:37
  181.4 1.0 slice.52
  182.6 0.7 slice_bitcast_fusion
  183.8 20.1 %all_to_all.52 = bf16[2,2,256]{2,1,0:T(2,128)(2,1)S(1)} all-to-all(bf16[2,2,256]{2,1,0:T(2,128)(2,1)S(1)} %reshape.321), channel_id=1, replica_groups=mesh['dp'=4,'kv_0'=8,'kv_1'=8,'tp'=2] {'tp'}, dimensions={0} | all-to-all | bytes 4096 | tf_op jit(solution)/shard_map/all_to_all | solution.py:84
  (85 shorter events, 7.0 us)
Async XLA Ops:
  0.6 79.9 %copy-start = (bf16[16,192,512]{2,1,0:T(8,128)(2,1)S(1)}, bf16[16,192,512]{2,1,0:T(8,128)(2,1)}, u32[]{:S(2)}) copy-start(bf16[16,192,512]{2,1,0:T(8,128)(2,1)} %param.23) | copy-start | bytes 9437188
  6.5 28.5 %all-to-all-start = ((f32[64,1,329]{2,1,0:T(1,128)}), f32[64,1,329]{2,1,0:T(1,128)S(1)}, u32[]{:S(2)}, u32[]{:S(2)}) async-start(f32[64,1,329]{2,1,0:T(1,128)} %all_to_all.32), calls=%async_computation | async-start | bytes 196608 | tf_op jit(solution)/shard_map/all_to_all | solution.py:54
  35.8 27.5 %copy-start.12 = (f32[512]{0:T(512)S(1)}, f32[512]{0:T(512)}, u32[]{:S(2)}) copy-start(f32[512]{0:T(512)} %param.19) | copy-start | bytes 6148
  35.8 16.1 %all-to-all-start.1 = ((f32[64,1,329]{2,1,0:T(1,128)}), f32[64,1,329]{2,1,0:T(1,128)S(1)}, u32[]{:S(2)}, u32[]{:S(2)}) async-start(f32[64,1,329]{2,1,0:T(1,128)} %broadcast_in_dim.82), calls=%async_computation.1 | async-start | bytes 196608 | tf_op jit(solution)/shard_map/all_to_all | solution.py:37
  57.7 16.2 %all-to-all-start.2 = ((bf16[64,2,512]{2,1,0:T(2,128)(2,1)}), bf16[64,2,512]{2,1,0:T(2,128)(2,1)S(1)}, u32[]{:S(2)}, u32[]{:S(2)}) async-start(bf16[64,2,512]{2,1,0:T(2,128)(2,1)} %reshape.315), calls=%async_computation.2 | async-start | bytes 262144 | tf_op jit(solution)/shard_map/all_to_all | solution.py:37
  62.5 15.6 %copy-start.6 = (bf16[16,16]{1,0:T(8,128)(2,1)}, bf16[16,16]{1,0:T(8,128)(2,1)S(1)}, u32[]{:S(2)}) copy-start(bf16[16,16]{1,0:T(8,128)(2,1)S(1)} %get-tuple-element.17) | copy-start | bytes 1540
  62.5 15.6 %copy-start.8 = (bf16[16,16]{1,0:T(8,128)(2,1)}, bf16[16,16]{1,0:T(8,128)(2,1)S(1)}, u32[]{:S(2)}) copy-start(bf16[16,16]{1,0:T(8,128)(2,1)S(1)} %get-tuple-element.18) | copy-start | bytes 1540
  62.7 0.6 copy-start.2
  62.7 0.6 copy-start.4
  79.6 1.9 copy-start.1
  79.6 1.9 copy-start.3
  79.6 1.9 copy-start.5
  133.1 8.5 %copy-start.11 = (bf16[8,512]{1,0:T(8,128)(2,1)S(1)}, bf16[8,512]{1,0:T(8,128)(2,1)}, u32[]{:S(2)}) copy-start(bf16[8,512]{1,0:T(8,128)(2,1)} %param.21) | copy-start | bytes 24580
  133.1 8.6 %copy-start.10 = (f32[16,8]{1,0:T(8,128)S(1)}, f32[16,8]{1,0:T(8,128)}, u32[]{:S(2)}) copy-start(f32[16,8]{1,0:T(8,128)} %get-tuple-element.5) | copy-start | bytes 1540
  135.2 34.9 %copy-start.7 = (bf16[16,16]{1,0:T(8,128)(2,1)S(1)}, bf16[16,16]{1,0:T(8,128)(2,1)}, u32[]{:S(2)}) copy-start(bf16[16,16]{1,0:T(8,128)(2,1)} %copy-done.6) | copy-start | bytes 1540
  135.2 34.9 %copy-start.9 = (bf16[16,16]{1,0:T(8,128)(2,1)S(1)}, bf16[16,16]{1,0:T(8,128)(2,1)}, u32[]{:S(2)}) copy-start(bf16[16,16]{1,0:T(8,128)(2,1)} %copy-done.8) | copy-start | bytes 1540
  137.1 46.4 %copy-start.13 = (bf16[512,64]{0,1:T(8,128)(2,1)S(1)}, bf16[512,64]{0,1:T(8,128)(2,1)}, u32[]{:S(2)}) copy-start(bf16[512,64]{0,1:T(8,128)(2,1)} %param.22) | copy-start | bytes 196612
  137.8 10.6 %all-to-all-start.4 = ((f32[8,1,1024]{2,1,0:T(1,128)}), f32[8,1,1024]{2,1,0:T(1,128)S(1)}, u32[]{:S(2)}, u32[]{:S(2)}) async-start(f32[8,1,1024]{2,1,0:T(1,128)} %reshape.319), calls=%async_computation.4 | async-start | bytes 65536 | tf_op jit(solution)/shard_map/all_to_all | solution.py:79
  165.5 15.7 %all-to-all-start.6 = ((f32[64,1,130]{2,1,0:T(1,128)}), f32[64,1,130]{2,1,0:T(1,128)S(1)}, u32[]{:S(2)}, u32[]{:S(2)}) async-start(f32[64,1,130]{2,1,0:T(1,128)} %broadcast_in_dim.87), calls=%async_computation.6 | async-start | bytes 131072 | tf_op jit(solution)/shard_map/all_to_all | solution.py:37
where the time goes:
time: 206 us; the launch traced here: 205 us
  blocking collectives  71.1 us (35%)
  waiting for transfers between devices  47.5 us (23%)
  starting transfers between devices  34.9 us (17%)
  local copies, waits for them, and re-layouts  30.3 us (15%)
  other arithmetic  12 us (6%)
  matrix products  7.86 us (4%)
    all_to_all x3, waiting for transfers between devices, sent_to_all(): lax.all_to_all(jnp.broadcast_to(value[None], (devices, *value.shape)), ax...  29.4 us
    all_to_all x2, blocking collectives, sent_and_summed(): lax.all_to_all(parts, axis, split_axis=0, concat_axis=0, tiled=True)  28 us
    pmax x2, blocking collectives, over_axes(): return functools.reduce(lax.pmax, axes, value)  23 us
    all_to_all x1, blocking collectives, summed_on_arrival(): lax.all_to_all(parts, axis, split_axis=0, concat_axis=0, tiled=True)  20.1 us
    all_to_all x1, starting transfers between devices, sent_and_summed(): lax.all_to_all(parts, axis, split_axis=0, concat_axis=0, tiled=True)  17.1 us
    unnamed x41, local copies, waits for them, and re-layouts  15.2 us
    all_to_all x3, starting transfers between devices, sent_to_all(): lax.all_to_all(jnp.broadcast_to(value[None], (devices, *value.shape)), ax...  14 us
    all_to_all x1, waiting for transfers between devices, sent_and_summed(): lax.all_to_all(parts, axis, split_axis=0, concat_axis=0, tiled=True)  11.4 us
  transfers between devices with their start and end apart: 5, of which 5 were waited for; matrix products, arithmetic and copies ran while one was open for 2% of the time, Pallas kernels for 0%

commit v1 on v0

v1 whole, which is shorter than its diff:
```python
import jax
import jax.numpy as jnp
from jax import lax
from jax.experimental import pallas as pl
from jax.experimental.pallas import tpu as pltpu
from jax.sharding import PartitionSpec as P

D = 4096
NOPE = 64
ROPE = 32
V_DIM = 64
RANK = 512
EPS = 1e-06
THETA = 10000.0
NEG = -1e30
SCALE = (NOPE + ROPE) ** (-0.5)
F32 = jnp.float32
BF16 = jnp.bfloat16
INTERPRET = False


def call(kernel, outs, *args, smem=(), scratch=()):
    specs = [
        pl.BlockSpec(memory_space=pltpu.SMEM if i in smem else pltpu.VMEM) for i in range(len(args))
    ]
    return pl.pallas_call(
        kernel,
        out_shape=tuple(jax.ShapeDtypeStruct(s, d) for s, d in outs),
        in_specs=specs,
        out_specs=tuple(pl.BlockSpec(memory_space=pltpu.VMEM) for _ in outs),
        scratch_shapes=list(scratch),
        interpret=INTERPRET,
    )(*args)


def split2(v):
    high = v.astype(BF16).astype(F32)
    return high, v - high


def split3(v):
    high, rest = split2(v)
    mid, low = split2(rest)
    return high, mid, low


def lanes(shape):
    return lax.broadcasted_iota(jnp.int32, shape, len(shape) - 1)


def project(x_ref, gain_ref, wn_ref, wr_ref, wl_ref, wk_ref, uk_ref, uv_ref, out_ref, buf):
    x = x_ref[...].astype(F32)
    scaled = (x * gain_ref[...]).astype(BF16)
    nope = jnp.dot(scaled, wn_ref[...], preferred_element_type=F32)
    rope = jnp.dot(scaled, wr_ref[...], preferred_element_type=F32)
    latent = jnp.dot(scaled, wl_ref[...], preferred_element_type=F32)
    key = jnp.dot(scaled, wk_ref[...], preferred_element_type=F32)
    squares = jnp.sum(x * x, axis=1, keepdims=True)
    first = lanes((8, 128)) < 64
    square_row = jnp.where(first, squares[:8], squares[8:])
    uk = uk_ref[...].astype(F32)
    uv = uv_ref[...].astype(F32)
    for h in range(8):
        at = pl.ds(8 * h, 8)
        n = slice(64 * h, 64 * h + 64)
        r = slice(32 * h, 32 * h + 32)
        c = slice(128 * (h // 2), 128 * (h // 2) + 128)
        s = slice(8 * (h % 2), 8 * (h % 2) + 8)
        weights = jnp.concatenate([uk[:, n], uv[:, n]], axis=1)
        buf[at, 0:8, :] = jnp.broadcast_to(weights[None], (8, 8, 128))
        rows = (
            jnp.concatenate([nope[:8, n], nope[8:, n]], axis=1),
            jnp.concatenate([rope[:8, r], key[:8], rope[8:, r], key[8:]], axis=1),
            latent[s, c],
            square_row,
        )
        for i, row in enumerate(rows):
            high, low = split2(row)
            buf[at, 8 + 2 * i, :] = high
            buf[at, 9 + 2 * i, :] = low
    out_ref[...] = buf[...].astype(BF16)


def queries(me_ref, got_ref, turn_ref, out_ref, w_ref, own_ref):
    got = got_ref[...].astype(F32)
    weights = got[:, 0:8, :].reshape(512, 128).astype(BF16)
    w_ref[...] = weights
    total = jnp.sum(got[:, 8:16, :], axis=0)
    nope = total[0:1] + total[1:2]
    rope = total[2:3] + total[3:4]
    latent = total[4:5] + total[5:6]
    inv_rms = lax.rsqrt((total[6:7] + total[7:8]) / D + EPS)
    lane = lanes((1, 128))
    q_low = (nope * inv_rms).astype(BF16).astype(F32)
    turned = pltpu.roll(q_low, 64, 1)
    row = lax.broadcasted_iota(jnp.int32, (8, 128), 0)
    wide = lanes((8, 128))
    q_wide = jnp.where(row < 4, jnp.broadcast_to(q_low, (8, 128)), jnp.broadcast_to(turned, (8, 128)))
    q_wide = jnp.where(wide < 64, q_wide, 0.0)
    q_latent = jnp.zeros((8, 128), F32)
    for c in range(4):
        left = jnp.where(row % 4 == c, q_wide, 0.0).astype(BF16)
        q_latent = q_latent + lax.dot_general(
            left,
            weights[128 * c : 128 * c + 128],
            (((1,), (1,)), ((), ())),
            preferred_element_type=F32,
        )
    turn = rope * inv_rms
    swapped = jnp.where(lane % 32 < 16, pltpu.roll(turn, 112, 1), pltpu.roll(turn, 16, 1))
    rotated = turn * turn_ref[0:1, :] + swapped * turn_ref[1:2, :]
    other = pltpu.roll(inv_rms, 64, 1)
    odd = (me_ref[0] // 8) % 2 == 1
    latent_rms = jnp.where((lane < 64) == odd, other, inv_rms)
    high, low = split2(latent * latent_rms)
    rest = jnp.concatenate([rotated, high, low, jnp.zeros((5, 128), F32)], axis=0)
    block = jnp.concatenate([q_latent, rest], axis=0).astype(BF16)
    own_ref[...] = block.astype(F32)
    out_ref[...] = jnp.broadcast_to(block[None], (64, 16, 128))


def attend(len_ref, me_ref, got_ref, cache_ref, rope_ref, out_ref, q_buf, r_buf, buf):
    for h in range(8):
        for j in range(8):
            piece = got_ref[8 * h + j].astype(F32)
            q_buf[j, :, h, :] = piece[0:8]
            r_buf[j, h : h + 1, :] = piece[8:9]
    base = me_ref[0] * 192
    position = lanes((8, 192)) + base
    first = lanes((8, 128)) < 64
    for j in range(8):
        for s in range(2):
            b = 8 * s + j
            q = jnp.concatenate([q_buf[j, 4 * s + c] for c in range(4)], axis=1).astype(BF16)
            q_rot = r_buf[j][:, 64 * s : 64 * s + 32].astype(BF16)
            keys = cache_ref[b]
            scores = lax.dot_general(
                q, keys, (((1,), (1,)), ((), ())), preferred_element_type=F32
            ) + jnp.dot(q_rot, rope_ref[b], preferred_element_type=F32)
            usable = position < len_ref[b]
            masked = jnp.where(usable, scores * SCALE, NEG)
            top = jnp.max(masked, axis=1, keepdims=True)
            weights = jnp.where(usable, jnp.exp(masked - top), 0.0)
            total = jnp.sum(weights, axis=1, keepdims=True)
            weighted = jnp.dot(weights.astype(BF16), keys, preferred_element_type=F32)
            for c in range(4):
                buf[:, j, 4 * s + c, :] = weighted[:, 128 * c : 128 * c + 128]
            for i, part in enumerate(split3(top)):
                buf[:, j, 8 + 4 * s + i, :] = jnp.broadcast_to(part, (8, 128))
            high, low = split2(total)
            buf[:, j, 11 + 4 * s, :] = jnp.where(first, high, low)
    out_ref[...] = buf[...].reshape(64, 16, 128).astype(BF16)


def new_entries(me_ref, got_ref, gain_ref, latent_ref, rope_ref, own_ref, buf):
    for src in range(64):
        piece = got_ref[src].astype(F32)
        c = src // 16
        b = src % 16
        buf[b : b + 1, 128 * c : 128 * c + 128] = piece[9:10] + piece[10:11]
        if src < 8:
            rope_ref[src : src + 1, :] = piece[8:9, 32:64]
            rope_ref[src + 8 : src + 9, :] = piece[8:9, 96:128]
    raw = buf[...]
    scale = lax.rsqrt(jnp.sum(raw * raw, axis=1, keepdims=True) / RANK + EPS)
    new = (raw * scale * gain_ref[...]).astype(BF16)
    latent_ref[...] = new
    buf[...] = new.astype(F32)
    j = me_ref[0] % 8
    for s in range(2):
        line = buf[pl.ds(j + 8 * s, 1), :]
        for c in range(4):
            own_ref[4 * s + c : 4 * s + c + 1, :] = line[:, 128 * c : 128 * c + 128]


def combine(got_ref, w_ref, own_q_ref, own_lat_ref, out_ref):
    got = got_ref[...].astype(F32)
    latent = own_lat_ref[...]
    query = own_q_ref[0:8, :]
    turned = own_q_ref[8:9, :]
    lane = lanes((1, 128))
    pair = turned * pltpu.roll(turned, 96, 1)
    dots = jnp.sum(query * latent, axis=1, keepdims=True)
    row = lax.broadcasted_iota(jnp.int32, (8, 128), 0)
    sums = []
    totals = []
    for s in range(2):
        here = (lane >= 64 * s) & (lane < 64 * s + 32)
        own = jnp.sum(dots[4 * s : 4 * s + 4], axis=0, keepdims=True) + jnp.sum(
            jnp.where(here, pair, 0.0), axis=1, keepdims=True
        )
        own = own * SCALE
        m = got[:, 8 + 4 * s, :] + got[:, 9 + 4 * s, :] + got[:, 10 + 4 * s, :]
        top = jnp.maximum(jnp.max(m, axis=0, keepdims=True), own)
        factor = jnp.exp(m - top)
        own_weight = jnp.exp(own - top)
        total = jnp.sum(factor * got[:, 11 + 4 * s, :], axis=0, keepdims=True)
        totals.append(total + pltpu.roll(total, 64, 1) + own_weight)
        own_low = own_weight.astype(BF16).astype(F32)
        sums.append(
            jnp.sum(got[:, 4 * s : 4 * s + 4, :] * factor[:, None, :], axis=0)
            + own_low * latent[4 * s : 4 * s + 4]
        )
    weighted_low = jnp.concatenate(sums, axis=0).astype(BF16)
    values = jnp.zeros((8, 128), F32)
    for c in range(4):
        part = jnp.dot(
            weighted_low, w_ref[128 * c : 128 * c + 128, :], preferred_element_type=F32
        )
        values = values + jnp.where(row % 4 == c, part, 0.0)
    front = jnp.sum(values[0:4], axis=0, keepdims=True) / totals[0]
    back = jnp.sum(values[4:8], axis=0, keepdims=True) / totals[1]
    attended = jnp.where(lane < 64, pltpu.roll(front, 64, 1), back).astype(BF16).astype(F32)
    out_ref[...] = jnp.broadcast_to(attended, (64, 128))


def output(tp_ref, got_ref, w_ref, keep_ref, send_ref):
    first = lanes((8, 128)) < 64
    total = jnp.zeros((16, 64), F32)
    for h in range(8):
        a = got_ref[8 * h : 8 * h + 8, :]
        left = jnp.concatenate([jnp.where(first, a, 0.0), jnp.where(first, 0.0, a)], axis=0)
        w = w_ref[64 * h : 64 * h + 64, :]
        total = total + jnp.dot(
            left.astype(BF16), jnp.concatenate([w, w], axis=0), preferred_element_type=F32
        )
    total = total.astype(BF16).astype(F32)
    low = total[:, :32]
    high = total[:, 32:]
    zero = tp_ref[0] == 0
    keep_ref[...] = jnp.where(zero, low, high)
    send_ref[...] = jnp.where(zero, high, low).astype(BF16)


def exchanged(value):
    return lax.all_to_all(value, "kv", split_axis=0, concat_axis=0, tiled=True)


def turn_rows(lengths, me):
    j = me % 8
    pair = jnp.stack([lengths[j], lengths[j + 8]]).astype(F32)
    inv_freq = THETA ** (-jnp.arange(ROPE // 2, dtype=F32) * 2.0 / ROPE)
    angles = pair[:, None] * inv_freq[None, :]
    cosine = jnp.cos(angles)
    sine = jnp.sin(angles)
    cosine = jnp.concatenate([cosine] * 4, axis=1).reshape(1, 128)
    sine = jnp.concatenate([-sine, sine, -sine, sine], axis=1).reshape(1, 128)
    return jnp.concatenate([cosine, sine], axis=0)


def local(
    token_state,
    norm_gain,
    wq_nope,
    wq_rope,
    w_latent,
    w_rope_key,
    kv_gain,
    w_uk,
    w_uv,
    w_out,
    latent_cache,
    rope_cache,
    lengths,
):
    me = lax.axis_index("kv").astype(jnp.int32)
    me_s = me.reshape(1)
    tp_s = lax.axis_index("tp").astype(jnp.int32).reshape(1)
    block = (64, 16, 128)
    (sent,) = call(
        project,
        [(block, BF16)],
        token_state,
        norm_gain.reshape(1, -1),
        wq_nope,
        wq_rope,
        w_latent,
        w_rope_key,
        w_uk,
        w_uv,
        scratch=[pltpu.VMEM(block, F32)],
    )
    sent, weights, own_q = call(
        queries,
        [(block, BF16), ((512, 128), BF16), ((16, 128), F32)],
        me_s,
        exchanged(sent),
        turn_rows(lengths, me),
        smem=(0,),
    )
    arrived = exchanged(sent)
    (sent,) = call(
        attend,
        [(block, BF16)],
        lengths,
        me_s,
        arrived,
        latent_cache,
        rope_cache,
        smem=(0, 1),
        scratch=[
            pltpu.VMEM((8, 8, 8, 128), F32),
            pltpu.VMEM((8, 8, 128), F32),
            pltpu.VMEM((8, 8, 16, 128), F32),
        ],
    )
    latent_new, rope_new, own_latent = call(
        new_entries,
        [((16, 512), BF16), ((16, 32), F32), ((8, 128), F32)],
        me_s,
        arrived,
        kv_gain.reshape(1, -1),
        smem=(0,),
        scratch=[pltpu.VMEM((16, 512), F32)],
    )
    (sent,) = call(combine, [((64, 128), F32)], exchanged(sent), weights, own_q, own_latent)
    arrived = exchanged(sent.reshape(64, 1, 128)).reshape(64, 128)
    keep, send = call(
        output, [((16, 32), F32), ((16, 32), BF16)], tp_s, arrived, w_out, smem=(0,)
    )
    other = lax.ppermute(send, "tp", [(0, 1), (1, 0)])
    mixed = (keep + other.astype(F32)).astype(BF16)
    return (mixed, latent_new, rope_new.astype(BF16))


def solution(mesh):
    in_specs = (
        P("dp", "kv"),
        P("kv"),
        P("kv", "tp"),
        P("kv", "tp"),
        P("kv", None),
        P("kv", None),
        P(),
        P("kv", "tp"),
        P("kv", "tp"),
        P("tp", "kv"),
        P("dp", "kv", None),
        P("dp", None, "kv"),
        P("dp"),
    )
    out_specs = (P("dp", ("kv", "tp")), P("dp", None), P("dp", None))
    return jax.shard_map(local, mesh=mesh, in_specs=in_specs, out_specs=out_specs, check_vma=False)
```

time: 206 us -> 112 us (0.54)
  blocking collectives: 71.1 us -> 18.3 us
  local copies, waits for them, and re-layouts: 30.3 us -> 5.66 us
  Pallas kernels: 0 us -> 18 us
  waiting for transfers between devices: 47.5 us -> 30 us
  matrix products: 7.86 us -> 0 us
  other arithmetic: 12 us -> 4.73 us
    all_to_all x3 -> x1, blocking collectives: 48.1 us -> 18.3 us  [exchanged(): return lax.all_to_all(value, 'kv', split_axis=0, concat_axis=0, tiled=True)]
    pmax x2 -> x0, blocking collectives: 23 us -> none  [over_axes(): return functools.reduce(lax.pmax, axes, value)]
    pallas_call x0 -> x6, Pallas kernels: none -> 18 us  [call(): pl.pallas_call(kernel, out_shape=tuple((jax.ShapeDtypeStruct(s, d) for s,...]
    all_to_all x5 -> x3, waiting for transfers between devices: 47.5 us -> 30 us  [exchanged(): return lax.all_to_all(value, 'kv', split_axis=0, concat_axis=0, tiled=True)]
    unnamed x41 -> x10, local copies, waits for them, and re-layouts: 15.2 us -> 4.17 us
    reshape x18 -> x2, local copies, waits for them, and re-layouts: 9.85 us -> 0.17 us  [the longest x1 0.08 us: turn_rows(): cosine = jnp.concatenate([cosine] * 4, axis=1).reshape(1, 128)]
    all_to_all x5 -> x3, starting transfers between devices: 34.9 us -> 26.3 us  [exchanged(): return lax.all_to_all(value, 'kv', split_axis=0, concat_axis=0, tiled=True)]
    ppermute x0 -> x1, starting transfers between devices: none -> 8.03 us  [local(): other = lax.ppermute(send, 'tp', [(0, 1), (1, 0)])]
  transfers between devices with their start and end apart: 5 -> 4, of which waited for: 5 -> 3; matrix products, arithmetic and copies ran while one was open for 2% -> 5% of each run, Pallas kernels for 0% -> 2%
where the time goes in v1:
time: 112 us
  starting transfers between devices  34.3 us (31%)
  waiting for transfers between devices  30 us (27%)
  blocking collectives  18.3 us (16%)
  Pallas kernels  18 us (16%)
  local copies, waits for them, and re-layouts  5.66 us (5%)
  other arithmetic  4.73 us (4%)
    all_to_all x3, waiting for transfers between devices, exchanged(): return lax.all_to_all(value, 'kv', split_axis=0, concat_axis=0, tiled=True)  30 us
    all_to_all x3, starting transfers between devices, exchanged(): return lax.all_to_all(value, 'kv', split_axis=0, concat_axis=0, tiled=True)  26.3 us
    all_to_all x1, blocking collectives, exchanged(): return lax.all_to_all(value, 'kv', split_axis=0, concat_axis=0, tiled=True)  18.3 us
    pallas_call x6, Pallas kernels, call(): pl.pallas_call(kernel, out_shape=tuple((jax.ShapeDtypeStruct(s, d) for s,...  18 us
    ppermute x1, starting transfers between devices, local(): other = lax.ppermute(send, 'tp', [(0, 1), (1, 0)])  8.03 us
    unnamed x10, local copies, waits for them, and re-layouts  4.17 us
  transfers between devices with their start and end apart: 4, of which 3 were waited for; matrix products, arithmetic and copies ran while one was open for 5% of the time, Pallas kernels for 2%

profile of v1, /device:TPU:1, one launch (start us, length us, event | category | flops | bytes accessed | tf_op | source)
XLA Modules:
  0.0 111.7 jit_solution(9909592816121804268)
XLA Ops:
  0.6 1.4 %copy.18.wk_ref = bf16[64,32]{1,0:T(8,128)(2,1)} copy(bf16[64,32]{0,1:T(8,128)(2,1)} %param.18) | data formatting | bytes 8192 | tf_op args[5]
  2.0 2.0 %shard_map.148 = bf16[64,16,128]{2,1,0:T(8,128)(2,1)} custom-call(bf16[16,64]{1,0:T(8,128)(2,1)} %x_ref.1, f32[1,64]{1,0:T(1,128)} %bitcast.11, bf16[64,512]{1,0:T(8,128)(2,1)} %wn_ref.1, bf16[64,256]{1,0:T(8,128)(2,1)} %wr_ref.1, bf16[64,512]{1,0:T(8,128)(2,1)} %wl_ref.1, bf16[64,32]{1,0:T(8,128)(2,1)} %copy.18.wk_ref, bf16[8,512]{1,0:T(8,128)(2,1)} %uk_ref.1, ...), custom_call_target="tpu_custom_call" | custom-call | tf_op jit(solution)/shard_map/pallas_call | solution.py:26
  4.0 17.1 %all-to-all-start = ((bf16[64,16,128]{2,1,0:T(8,128)(2,1)}), bf16[64,16,128]{2,1,0:T(8,128)(2,1)S(1)}, u32[]{:S(2)}, u32[]{:S(2)}) async-start(bf16[64,16,128]{2,1,0:T(8,128)(2,1)} %shard_map.148), calls=%async_computation | async-start | bytes 524288 | tf_op jit(solution)/shard_map/all_to_all | solution.py:236
  21.1 0.0 copy-start.3
  21.2 1.3 %fusion.1 = (s32[1]{0:T(128)}, s32[1]{0:T(128)}) fusion(s32[16]{0:T(128)} %len_ref.1, s32[]{:T(128)S(6)} %select_n.14, s32[]{:T(128)S(6)} %select_n.15), kind=kLoop, calls=%fused_computation.9 | loop fusion | bytes 24 | tf_op jit(solution)/shard_map/dynamic_slice | solution.py:241
  22.5 1.4 %add_convert_fusion.1 = f32[2]{0:T(128)S(1)} fusion(s32[1]{0:T(128)} %get-tuple-element.23, s32[1]{0:T(128)} %get-tuple-element.22), kind=kLoop, calls=%fused_computation.6 | loop fusion | flops 4 | bytes 16 | tf_op jit(solution)/shard_map/convert_element_type | solution.py:241
  23.8 0.1 multiply_cosine_fusion
  24.0 0.1 pad_maximum_fusion
  24.0 0.1 reshape.54
  24.1 0.1 reshape.55
  24.2 0.6 pad_maximum_fusion.2.turn_ref
  24.8 9.2 %all-to-all-done.got_ref = bf16[64,16,128]{2,1,0:T(8,128)(2,1)S(1)} async-done(((bf16[64,16,128]{2,1,0:T(8,128)(2,1)}), bf16[64,16,128]{2,1,0:T(8,128)(2,1)S(1)}, u32[]{:S(2)}, u32[]{:S(2)}) %all-to-all-start) | async-done | bytes 262176 | tf_op jit(solution)/shard_map/all_to_all | solution.py:236
  33.9 0.0 copy-start
  33.9 0.7 copy-done
  34.6 2.0 %shard_map.149 = (bf16[64,16,128]{2,1,0:T(8,128)(2,1)}, bf16[512,128]{1,0:T(8,128)(2,1)}, f32[16,128]{1,0:T(8,128)}) custom-call(s32[1]{0:T(128)} %bitcast.1.me_ref, bf16[64,16,128]{2,1,0:T(8,128)(2,1)} %copy-done, f32[2,128]{1,0:T(2,128)} %pad_maximum_fusion.2.turn_ref), custom_call_target="tpu_custom_call" | custom-call | tf_op jit(solution)/shard_map/pallas_call | solution.py:26
  36.6 18.3 %all_to_all.20.got_ref = bf16[64,16,128]{2,1,0:T(8,128)(2,1)} all-to-all(bf16[64,16,128]{2,1,0:T(8,128)(2,1)} %get-tuple-element.11), channel_id=1, replica_groups=mesh['dp'=4,'kv'=64,'tp'=2] {'kv'}, dimensions={0} | all-to-all | bytes 524288 | tf_op jit(solution)/shard_map/all_to_all | solution.py:236
  54.9 8.3 %shard_map.150 = bf16[64,16,128]{2,1,0:T(8,128)(2,1)} custom-call(s32[16]{0:T(128)} %len_ref.1, s32[1]{0:T(128)} %bitcast.1.me_ref, bf16[64,16,128]{2,1,0:T(8,128)(2,1)} %all_to_all.20.got_ref, bf16[16,192,512]{2,1,0:T(8,128)(2,1)} %cache_ref.1, bf16[16,32,192]{2,1,0:T(8,128)(2,1)} %rope_ref.1), custom_call_target="tpu_custom_call" | custom-call | tf_op jit(solution)/shard_map/pallas_call | solution.py:26
  63.2 4.6 %all-to-all-start.2 = ((bf16[64,16,128]{2,1,0:T(8,128)(2,1)}), bf16[64,16,128]{2,1,0:T(8,128)(2,1)S(1)}, u32[]{:S(2)}, u32[]{:S(2)}) async-start(bf16[64,16,128]{2,1,0:T(8,128)(2,1)} %shard_map.150), calls=%async_computation.2 | async-start | bytes 524288 | tf_op jit(solution)/shard_map/all_to_all | solution.py:236
  67.8 1.7 %shard_map.151 = (bf16[16,512]{1,0:T(8,128)(2,1)}, f32[16,32]{1,0:T(8,128)}, f32[8,128]{1,0:T(8,128)}) custom-call(s32[1]{0:T(128)} %bitcast.1.me_ref, bf16[64,16,128]{2,1,0:T(8,128)(2,1)} %all_to_all.20.got_ref, f32[1,512]{1,0:T(1,128)} %bitcast.10), custom_call_target="tpu_custom_call" | custom-call | tf_op jit(solution)/shard_map/pallas_call | solution.py:26
  69.5 10.8 %all-to-all-done.2.got_ref = bf16[64,16,128]{2,1,0:T(8,128)(2,1)S(1)} async-done(((bf16[64,16,128]{2,1,0:T(8,128)(2,1)}), bf16[64,16,128]{2,1,0:T(8,128)(2,1)S(1)}, u32[]{:S(2)}, u32[]{:S(2)}) %all-to-all-start.2) | async-done | bytes 262176 | tf_op jit(solution)/shard_map/all_to_all | solution.py:236
  80.3 0.0 copy-start.1
  80.3 0.7 copy-done.1
  81.0 2.2 %shard_map.152 = f32[64,128]{1,0:T(8,128)} custom-call(bf16[64,16,128]{2,1,0:T(8,128)(2,1)} %copy-done.1, bf16[512,128]{1,0:T(8,128)(2,1)} %get-tuple-element.12.w_ref, f32[16,128]{1,0:T(8,128)} %get-tuple-element.13.own_q_ref, f32[8,128]{1,0:T(8,128)} %get-tuple-element.14.own_lat_ref), custom_call_target="tpu_custom_call" | custom-call | tf_op jit(solution)/shard_map/pallas_call | solution.py:26
  83.2 4.5 %all-to-all-start.3 = ((f32[64,1,128]{2,1,0:T(1,128)}), f32[64,1,128]{2,1,0:T(1,128)S(1)}, u32[]{:S(2)}, u32[]{:S(2)}) async-start(f32[64,1,128]{2,1,0:T(1,128)} %bitcast.9), calls=%async_computation.3 | async-start | bytes 65536 | tf_op jit(solution)/shard_map/all_to_all | solution.py:236
  87.7 0.0 copy-done.3
  87.8 0.8 copy.20.w_ref
  88.5 10.1 %all-to-all-done.3 = f32[64,1,128]{2,1,0:T(1,128)S(1)} async-done(((f32[64,1,128]{2,1,0:T(1,128)}), f32[64,1,128]{2,1,0:T(1,128)S(1)}, u32[]{:S(2)}, u32[]{:S(2)}) %all-to-all-start.3) | async-done | bytes 32800 | tf_op jit(solution)/shard_map/all_to_all | solution.py:236
  98.6 0.0 copy-start.2
  98.6 0.6 copy-done.2
  99.2 1.8 %shard_map.153 = (f32[16,32]{1,0:T(8,128)}, bf16[16,32]{1,0:T(8,128)(2,1)}) custom-call(s32[1]{0:T(128)} %bitcast.tp_ref, f32[64,128]{1,0:T(8,128)} %bitcast.8, bf16[512,64]{1,0:T(8,128)(2,1)} %copy.20.w_ref), custom_call_target="tpu_custom_call" | custom-call | tf_op jit(solution)/shard_map/pallas_call | solution.py:26
  101.1 8.0 %collective-permute-start = (bf16[16,32]{1,0:T(8,128)(2,1)}, bf16[16,32]{1,0:T(8,128)(2,1)S(1)}, u32[]{:S(2)}, u32[]{:S(2)}) collective-permute-start(bf16[16,32]{1,0:T(8,128)(2,1)} %get-tuple-element.16), channel_id=1, source_target_pairs={{0,1},{1,0},{2,3},{3,2},{4,5},{5,4},{6,7},{7,6},{8,9},{9,8},{10,11... | collective-permute-start | bytes 3080 | tf_op jit(solution)/shard_map/ppermute | solution.py:321
  109.1 1.3 %convert_element_type.19 = bf16[16,32]{1,0:T(8,128)(2,1)} convert(f32[16,32]{1,0:T(8,128)} %get-tuple-element.18) | non-fusion elementwise | flops 512 | bytes 3072 | tf_op jit(solution)/shard_map/convert_element_type | solution.py:323
  110.4 0.0 collective-permute-done
  110.4 1.3 %add_convert_fusion = bf16[16,32]{1,0:T(8,128)(2,1)} fusion(f32[16,32]{1,0:T(8,128)} %get-tuple-element.15, bf16[16,32]{1,0:T(8,128)(2,1)S(1)} %collective-permute-done), kind=kLoop, calls=%fused_computation | loop fusion | flops 1536 | bytes 4096 | tf_op jit(solution)/shard_map/convert_element_type | solution.py:322
  (1 shorter events, 0.0 us)
Async XLA Ops:
  4.0 30.0 %all-to-all-start = ((bf16[64,16,128]{2,1,0:T(8,128)(2,1)}), bf16[64,16,128]{2,1,0:T(8,128)(2,1)S(1)}, u32[]{:S(2)}, u32[]{:S(2)}) async-start(bf16[64,16,128]{2,1,0:T(8,128)(2,1)} %shard_map.148), calls=%async_computation | async-start | bytes 524288 | tf_op jit(solution)/shard_map/all_to_all | solution.py:236
  21.1 66.6 %copy-start.3 = (bf16[512,64]{0,1:T(8,128)(2,1)S(1)}, bf16[512,64]{0,1:T(8,128)(2,1)}, u32[]{:S(2)}) copy-start(bf16[512,64]{0,1:T(8,128)(2,1)} %param.22) | copy-start | bytes 196612
  33.9 0.7 copy-start
  63.2 17.1 %all-to-all-start.2 = ((bf16[64,16,128]{2,1,0:T(8,128)(2,1)}), bf16[64,16,128]{2,1,0:T(8,128)(2,1)S(1)}, u32[]{:S(2)}, u32[]{:S(2)}) async-start(bf16[64,16,128]{2,1,0:T(8,128)(2,1)} %shard_map.150), calls=%async_computation.2 | async-start | bytes 524288 | tf_op jit(solution)/shard_map/all_to_all | solution.py:236
  80.3 0.7 copy-start.1
  83.2 15.4 %all-to-all-start.3 = ((f32[64,1,128]{2,1,0:T(1,128)}), f32[64,1,128]{2,1,0:T(1,128)S(1)}, u32[]{:S(2)}, u32[]{:S(2)}) async-start(f32[64,1,128]{2,1,0:T(1,128)} %bitcast.9), calls=%async_computation.3 | async-start | bytes 65536 | tf_op jit(solution)/shard_map/all_to_all | solution.py:236
  98.6 0.6 copy-start.2
  101.1 9.3 %collective-permute-start = (bf16[16,32]{1,0:T(8,128)(2,1)}, bf16[16,32]{1,0:T(8,128)(2,1)S(1)}, u32[]{:S(2)}, u32[]{:S(2)}) collective-permute-start(bf16[16,32]{1,0:T(8,128)(2,1)} %get-tuple-element.16), channel_id=1, source_target_pairs={{0,1},{1,0},{2,3},{3,2},{4,5},{5,4},{6,7},{7,6},{8,9},{9,8},{10,11... | collective-permute-start | bytes 3080 | tf_op jit(solution)/shard_map/ppermute | solution.py:321

commit v2 on v1

--- a/solution.py
+++ b/solution.py
@@ -19,18 +19,36 @@
 INTERPRET = False
 
 
-def call(kernel, outs, *args, smem=(), scratch=()):
-    specs = [
-        pl.BlockSpec(memory_space=pltpu.SMEM if i in smem else pltpu.VMEM) for i in range(len(args))
+def call(kernel, outs, *args, smem=(), near=(), far=(), results_far=(), scratch=()):
+    spaces = [
+        pltpu.SMEM if i in smem else pl.ANY if i in far else pltpu.VMEM for i in range(len(args))
     ]
-    return pl.pallas_call(
-        kernel,
-        out_shape=tuple(jax.ShapeDtypeStruct(s, d) for s, d in outs),
-        in_specs=specs,
-        out_specs=tuple(pl.BlockSpec(memory_space=pltpu.VMEM) for _ in outs),
+    body = kernel
+    shapes = [
+        jax.ShapeDtypeStruct(*out) if i in results_far else pltpu.VMEM(*out)
+        for i, out in enumerate(outs)
+    ]
+    if len(outs) == 1 and not results_far:
+        shapes.append(pltpu.VMEM((8, 128), F32))
+
+        def body(*refs):
+            refs[len(args) + 1][...] = jnp.zeros((8, 128), F32)
+            kernel(*refs[: len(args) + 1], *refs[len(args) + 2 :])
+
+    results = pl.pallas_call(
+        body,
+        out_shape=tuple(shapes),
+        in_specs=[pl.BlockSpec(memory_space=space) for space in spaces],
+        out_specs=tuple(pl.BlockSpec(memory_space=pltpu.VMEM) for _ in shapes),
         scratch_shapes=list(scratch),
         interpret=INTERPRET,
-    )(*args)
+    )(
+        *(
+            pltpu.with_memory_space_constraint(a, pltpu.VMEM) if i in near else a
+            for i, a in enumerate(args)
+        )
+    )
+    return results[: len(outs)]
 
 
 def split2(v):
@@ -54,7 +72,9 @@
     nope = jnp.dot(scaled, wn_ref[...], preferred_element_type=F32)
     rope = jnp.dot(scaled, wr_ref[...], preferred_element_type=F32)
     latent = jnp.dot(scaled, wl_ref[...], preferred_element_type=F32)
-    key = jnp.dot(scaled, wk_ref[...], preferred_element_type=F32)
+    key = lax.dot_general(
+        scaled, wk_ref[...], (((1,), (1,)), ((), ())), preferred_element_type=F32
+    )
     squares = jnp.sum(x * x, axis=1, keepdims=True)
     first = lanes((8, 128)) < 64
     square_row = jnp.where(first, squares[:8], squares[8:])
@@ -119,7 +139,22 @@
     out_ref[...] = jnp.broadcast_to(block[None], (64, 16, 128))
 
 
-def attend(len_ref, me_ref, got_ref, cache_ref, rope_ref, out_ref, q_buf, r_buf, buf):
+def attend(
+    len_ref, me_ref, got_ref, cache_hbm, rope_hbm, out_ref, q_buf, r_buf, buf, cache_ref, rope_ref, sem
+):
+    copies = []
+    for j in range(8):
+        for s in range(2):
+            b = 8 * s + j
+            copies.append(
+                (
+                    pltpu.make_async_copy(cache_hbm.at[b], cache_ref.at[b], sem.at[0, b]),
+                    pltpu.make_async_copy(rope_hbm.at[b], rope_ref.at[b], sem.at[1, b]),
+                )
+            )
+    for pair in copies:
+        for copy in pair:
+            copy.start()
     for h in range(8):
         for j in range(8):
             piece = got_ref[8 * h + j].astype(F32)
@@ -133,6 +168,8 @@
             b = 8 * s + j
             q = jnp.concatenate([q_buf[j, 4 * s + c] for c in range(4)], axis=1).astype(BF16)
             q_rot = r_buf[j][:, 64 * s : 64 * s + 32].astype(BF16)
+            for copy in copies[2 * j + s]:
+                copy.wait()
             keys = cache_ref[b]
             scores = lax.dot_general(
                 q, keys, (((1,), (1,)), ((), ())), preferred_element_type=F32
@@ -152,15 +189,18 @@
     out_ref[...] = buf[...].reshape(64, 16, 128).astype(BF16)
 
 
-def new_entries(me_ref, got_ref, gain_ref, latent_ref, rope_ref, own_ref, buf):
+def new_entries(
+    me_ref, tp_ref, got_ref, gain_ref, w_ref, latent_ref, rope_ref, own_ref, half_ref, buf, turn_buf
+):
     for src in range(64):
         piece = got_ref[src].astype(F32)
         c = src // 16
         b = src % 16
         buf[b : b + 1, 128 * c : 128 * c + 128] = piece[9:10] + piece[10:11]
         if src < 8:
-            rope_ref[src : src + 1, :] = piece[8:9, 32:64]
-            rope_ref[src + 8 : src + 9, :] = piece[8:9, 96:128]
+            turn_buf[src : src + 1, :] = piece[8:9]
+    turned = turn_buf[...]
+    rope_ref[...] = jnp.concatenate([turned[:, 32:64], turned[:, 96:128]], axis=0).astype(BF16)
     raw = buf[...]
     scale = lax.rsqrt(jnp.sum(raw * raw, axis=1, keepdims=True) / RANK + EPS)
     new = (raw * scale * gain_ref[...]).astype(BF16)
@@ -171,6 +211,7 @@
         line = buf[pl.ds(j + 8 * s, 1), :]
         for c in range(4):
             own_ref[4 * s + c : 4 * s + c + 1, :] = line[:, 128 * c : 128 * c + 128]
+    half_ref[...] = jnp.where(tp_ref[0] == 0, w_ref[32:64, :], w_ref[0:32, :])
 
 
 def combine(got_ref, w_ref, own_q_ref, own_lat_ref, out_ref):
@@ -211,29 +252,33 @@
     front = jnp.sum(values[0:4], axis=0, keepdims=True) / totals[0]
     back = jnp.sum(values[4:8], axis=0, keepdims=True) / totals[1]
     attended = jnp.where(lane < 64, pltpu.roll(front, 64, 1), back).astype(BF16).astype(F32)
-    out_ref[...] = jnp.broadcast_to(attended, (64, 128))
-
-
-def output(tp_ref, got_ref, w_ref, keep_ref, send_ref):
+    out_ref[...] = jnp.broadcast_to(attended, (128, 128))
+
+
+def output(tp_ref, got_ref, w_ref, other_ref, out_ref):
     first = lanes((8, 128)) < 64
-    total = jnp.zeros((16, 64), F32)
-    for h in range(8):
-        a = got_ref[8 * h : 8 * h + 8, :]
-        left = jnp.concatenate([jnp.where(first, a, 0.0), jnp.where(first, 0.0, a)], axis=0)
-        w = w_ref[64 * h : 64 * h + 64, :]
-        total = total + jnp.dot(
-            left.astype(BF16), jnp.concatenate([w, w], axis=0), preferred_element_type=F32
-        )
-    total = total.astype(BF16).astype(F32)
-    low = total[:, :32]
-    high = total[:, 32:]
-    zero = tp_ref[0] == 0
-    keep_ref[...] = jnp.where(zero, low, high)
-    send_ref[...] = jnp.where(zero, high, low).astype(BF16)
-
-
-def exchanged(value):
-    return lax.all_to_all(value, "kv", split_axis=0, concat_axis=0, tiled=True)
+    tp = tp_ref[0]
+    mixed = jnp.zeros((16, 32), F32)
+    for group in range(2):
+        pieces = []
+        for pair in range(4):
+            even = got_ref[pl.ds(32 * pair + group, 8, stride=2), :]
+            odd = got_ref[pl.ds(32 * pair + 16 + group, 8, stride=2), :]
+            front = jnp.where(first, even, pltpu.roll(odd, 64, 1))
+            back = jnp.where(first, pltpu.roll(even, 64, 1), odd)
+            pieces.append(jnp.concatenate([front, back], axis=0))
+        attended = jnp.concatenate(pieces, axis=1).astype(BF16)
+        mine = jnp.where(tp == 0, w_ref[0:32, :], w_ref[32:64, :])
+        w = jnp.where(tp == group, mine, other_ref[...])
+        part = lax.dot_general(
+            attended, w, (((1,), (1,)), ((), ())), preferred_element_type=F32
+        )
+        mixed = mixed + part.astype(BF16).astype(F32)
+    out_ref[...] = mixed.astype(BF16)
+
+
+def exchanged(value, axes="kv"):
+    return lax.all_to_all(value, axes, split_axis=0, concat_axis=0, tiled=True)
 
 
 def turn_rows(lengths, me):
@@ -275,7 +320,7 @@
         wq_nope,
         wq_rope,
         w_latent,
-        w_rope_key,
+        w_rope_key.T,
         w_uk,
         w_uv,
         scratch=[pltpu.VMEM(block, F32)],
@@ -287,6 +332,7 @@
         exchanged(sent),
         turn_rows(lengths, me),
         smem=(0,),
+        near=(1, 2),
     )
     arrived = exchanged(sent)
     (sent,) = call(
@@ -298,29 +344,53 @@
         latent_cache,
         rope_cache,
         smem=(0, 1),
+        near=(2,),
+        far=(3, 4),
         scratch=[
             pltpu.VMEM((8, 8, 8, 128), F32),
             pltpu.VMEM((8, 8, 128), F32),
             pltpu.VMEM((8, 8, 16, 128), F32),
+            pltpu.VMEM((16, 192, 512), BF16),
+            pltpu.VMEM((16, 32, 192), BF16),
+            pltpu.SemaphoreType.DMA((2, 16)),
         ],
     )
-    latent_new, rope_new, own_latent = call(
+    latent_new, rope_new, own_latent, half = call(
         new_entries,
-        [((16, 512), BF16), ((16, 32), F32), ((8, 128), F32)],
+        [((16, 512), BF16), ((16, 32), BF16), ((8, 128), F32), ((32, 512), BF16)],
         me_s,
+        tp_s,
         arrived,
         kv_gain.reshape(1, -1),
+        w_out.T,
+        smem=(0, 1),
+        near=(2,),
+        results_far=(0, 1),
+        scratch=[pltpu.VMEM((16, 512), F32), pltpu.VMEM((8, 128), F32)],
+    )
+    other = lax.ppermute(half, "tp", [(0, 1), (1, 0)])
+    (sent,) = call(
+        combine,
+        [((128, 128), F32)],
+        exchanged(sent),
+        weights,
+        own_q,
+        own_latent,
+        near=(0, 1, 2, 3),
+    )
+    arrived = exchanged(sent.reshape(128, 1, 128), ("kv", "tp")).reshape(128, 128)
+    (mixed,) = call(
+        output,
+        [((16, 32), BF16)],
+        tp_s,
+        arrived,
+        w_out.T,
+        other,
         smem=(0,),
-        scratch=[pltpu.VMEM((16, 512), F32)],
-    )
-    (sent,) = call(combine, [((64, 128), F32)], exchanged(sent), weights, own_q, own_latent)
-    arrived = exchanged(sent.reshape(64, 1, 128)).reshape(64, 128)
-    keep, send = call(
-        output, [((16, 32), F32), ((16, 32), BF16)], tp_s, arrived, w_out, smem=(0,)
-    )
-    other = lax.ppermute(send, "tp", [(0, 1), (1, 0)])
-    mixed = (keep + other.astype(F32)).astype(BF16)
-    return (mixed, latent_new, rope_new.astype(BF16))
+        near=(1, 3),
+        results_far=(0,),
+    )
+    return (mixed, latent_new, rope_new)
 
 
 def solution(mesh):

time: 112 us -> 103 us (0.920)
  local copies, waits for them, and re-layouts: 5.66 us -> 1.49 us
  other arithmetic: 4.73 us -> 1.58 us
    all_to_all x3, starting transfers between devices: 26.3 us -> 31.5 us  [exchanged(): return lax.all_to_all(value, axes, split_axis=0, concat_axis=0, tiled=True)]
    ppermute x1, starting transfers between devices: 8.03 us -> 2.91 us  [local(): other = lax.ppermute(half, 'tp', [(0, 1), (1, 0)])]
    unnamed x10 -> x0, local copies, waits for them, and re-layouts: 4.17 us -> none
    convert_element_type x2 -> x0, other arithmetic: 2.59 us -> none  [the longest x1 1.29 us: local(): mixed = (keep + other.astype(F32)).astype(BF16)]
    all_to_all x3, waiting for transfers between devices: 30 us -> 28.5 us  [exchanged(): return lax.all_to_all(value, axes, split_axis=0, concat_axis=0, tiled=True)]
  transfers between devices with their start and end apart: 4 -> 4, of which waited for: 3 -> 4; matrix products, arithmetic and copies ran while one was open for 5% -> 3% of each run, Pallas kernels for 2% -> 2%
where the time goes in v2:
time: 103 us
  starting transfers between devices  34.5 us (33%)
  waiting for transfers between devices  29.3 us (28%)
  blocking collectives  17.9 us (17%)
  Pallas kernels  17.1 us (17%)
  other arithmetic  1.58 us (2%)
  local copies, waits for them, and re-layouts  1.49 us (1%)
    all_to_all x3, starting transfers between devices, exchanged(): return lax.all_to_all(value, axes, split_axis=0, concat_axis=0, tiled=True)  31.5 us
    all_to_all x3, waiting for transfers between devices, exchanged(): return lax.all_to_all(value, axes, split_axis=0, concat_axis=0, tiled=True)  28.5 us
    all_to_all x1, blocking collectives, exchanged(): return lax.all_to_all(value, axes, split_axis=0, concat_axis=0, tiled=True)  17.9 us
    pallas_call x6, Pallas kernels, call(): pl.pallas_call(body, out_shape=tuple(shapes), in_specs=[pl.BlockSpec(memo...  17.1 us
    ppermute x1, starting transfers between devices, local(): other = lax.ppermute(half, 'tp', [(0, 1), (1, 0)])  2.91 us
  transfers between devices with their start and end apart: 4, of which 4 were waited for; matrix products, arithmetic and copies ran while one was open for 3% of the time, Pallas kernels for 2%

profile of v2, /device:TPU:1, one launch (start us, length us, event | category | flops | bytes accessed | tf_op | source)
XLA Modules:
  0.0 102.6 jit_solution(1216492188462271200)
XLA Ops:
  0.6 2.0 %shard_map.148 = (bf16[64,16,128]{2,1,0:T(8,128)(2,1)}, f32[8,128]{1,0:T(8,128)}) custom-call(bf16[16,64]{1,0:T(8,128)(2,1)} %refs_0_.2, f32[1,64]{1,0:T(1,128)} %bitcast.15, bf16[64,512]{1,0:T(8,128)(2,1)} %refs_2_.1, bf16[64,256]{1,0:T(8,128)(2,1)} %refs_3_.2, bf16[64,512]{1,0:T(8,128)(2,1)} %refs_4_.2, bf16[32,64]{1,0:T(8,128)(2,1)} %bitcast.13, ...), custom_call_target="tpu_custom_call" | custom-call | tf_op jit(solution)/shard_map/pallas_call | solution.py:38
  2.6 17.1 %all-to-all-start = ((bf16[64,16,128]{2,1,0:T(8,128)(2,1)}), bf16[64,16,128]{2,1,0:T(8,128)(2,1)S(1)}, u32[]{:S(2)}, u32[]{:S(2)}) async-start(bf16[64,16,128]{2,1,0:T(8,128)(2,1)} %get-tuple-element.13), calls=%async_computation | async-start | bytes 524288 | tf_op jit(solution)/shard_map/all_to_all | solution.py:281
  19.8 1.3 %fusion.1 = (s32[1]{0:T(128)}, s32[1]{0:T(128)}) fusion(s32[16]{0:T(128)} %refs_0_.3, s32[]{:T(128)S(6)} %select_n.14, s32[]{:T(128)S(6)} %select_n.15), kind=kLoop, calls=%fused_computation.8 | loop fusion | bytes 24 | tf_op jit(solution)/shard_map/dynamic_slice | solution.py:286
  21.1 1.4 %add_convert_fusion = f32[2]{0:T(128)S(1)} fusion(s32[1]{0:T(128)} %get-tuple-element.27, s32[1]{0:T(128)} %get-tuple-element.26), kind=kLoop, calls=%fused_computation.5 | loop fusion | flops 4 | bytes 16 | tf_op jit(solution)/shard_map/convert_element_type | solution.py:286
  22.5 0.1 multiply_cosine_fusion
  22.6 0.1 pad_maximum_fusion
  22.7 0.1 reshape.54
  22.7 0.1 reshape.55
  22.8 9.7 %all-to-all-done.got_ref = bf16[64,16,128]{2,1,0:T(8,128)(2,1)S(1)} async-done(((bf16[64,16,128]{2,1,0:T(8,128)(2,1)}), bf16[64,16,128]{2,1,0:T(8,128)(2,1)S(1)}, u32[]{:S(2)}, u32[]{:S(2)}) %all-to-all-start) | async-done | bytes 262176 | tf_op jit(solution)/shard_map/all_to_all | solution.py:281
  32.6 0.3 shard_map.149
  32.9 17.9 %all_to_all.20.refs_2_.got_ref = bf16[64,16,128]{2,1,0:T(8,128)(2,1)S(1)} all-to-all(bf16[64,16,128]{2,1,0:T(8,128)(2,1)S(1)} %get-tuple-element.14), channel_id=1, replica_groups=mesh['dp'=4,'kv'=64,'tp'=2] {'kv'}, dimensions={0} | all-to-all | bytes 524288 | tf_op jit(solution)/shard_map/all_to_all | solution.py:281
  50.8 10.4 %shard_map.150 = (bf16[64,16,128]{2,1,0:T(8,128)(2,1)}, f32[8,128]{1,0:T(8,128)}) custom-call(s32[16]{0:T(128)} %refs_0_.3, s32[1]{0:T(128)} %bitcast.1.me_ref.refs_1_, bf16[64,16,128]{2,1,0:T(8,128)(2,1)S(1)} %all_to_all.20.refs_2_.got_ref, bf16[16,192,512]{2,1,0:T(8,128)(2,1)} %refs_3_.3, bf16[16,32,192]{2,1,0:T(8,128)(2,1)} %refs_4_.3), custom_call_target="tpu_custom_call" | custom-call | tf_op jit(solution)/shard_map/pallas_call | solution.py:38
  61.3 5.7 %all-to-all-start.2 = ((bf16[64,16,128]{2,1,0:T(8,128)(2,1)}), bf16[64,16,128]{2,1,0:T(8,128)(2,1)S(1)}, u32[]{:S(2)}, u32[]{:S(2)}) async-start(bf16[64,16,128]{2,1,0:T(8,128)(2,1)} %get-tuple-element.15), calls=%async_computation.2 | async-start | bytes 524288 | tf_op jit(solution)/shard_map/all_to_all | solution.py:281
  67.0 1.6 %shard_map.151 = (bf16[16,512]{1,0:T(8,128)(2,1)}, bf16[16,32]{1,0:T(8,128)(2,1)}, f32[8,128]{1,0:T(8,128)S(1)}, bf16[32,512]{1,0:T(8,128)(2,1)S(1)}) custom-call(s32[1]{0:T(128)} %bitcast.1.me_ref.refs_1_, s32[1]{0:T(128)} %bitcast.tp_ref, bf16[64,16,128]{2,1,0:T(8,128)(2,1)S(1)} %all_to_all.20.refs_2_.got_ref, f32[1,512]{1,0:T(1,128)} %bitcast.14, ...), custom_call_target="tpu_custom_call" | custom-call | tf_op jit(solution)/shard_map/pallas_call | solution.py:38
  68.6 10.9 %all-to-all-done.2.refs_0_ = bf16[64,16,128]{2,1,0:T(8,128)(2,1)S(1)} async-done(((bf16[64,16,128]{2,1,0:T(8,128)(2,1)}), bf16[64,16,128]{2,1,0:T(8,128)(2,1)S(1)}, u32[]{:S(2)}, u32[]{:S(2)}) %all-to-all-start.2) | async-done | bytes 262176 | tf_op jit(solution)/shard_map/all_to_all | solution.py:281
  79.5 1.2 %shard_map.152 = (f32[128,128]{1,0:T(8,128)}, f32[8,128]{1,0:T(8,128)}) custom-call(bf16[64,16,128]{2,1,0:T(8,128)(2,1)S(1)} %all-to-all-done.2.refs_0_, bf16[512,128]{1,0:T(8,128)(2,1)S(1)} %get-tuple-element.16.refs_1_, f32[16,128]{1,0:T(8,128)S(1)} %get-tuple-element.17.refs_2_, f32[8,128]{1,0:T(8,128)S(1)} %get-tuple-element.18.refs_3_), custom_call_target="tpu_custom_call" | custom-call | tf_op jit(solution)/shard_map/pallas_call | solution.py:38
  80.7 8.7 %all-to-all-start.3 = ((f32[128,1,128]{2,1,0:T(1,128)}), f32[128,1,128]{2,1,0:T(1,128)S(1)}, u32[]{:S(2)}, u32[]{:S(2)}) async-start(f32[128,1,128]{2,1,0:T(1,128)} %bitcast.7), calls=%async_computation.3 | async-start | bytes 131072 | tf_op jit(solution)/shard_map/all_to_all | solution.py:281
  89.4 2.9 %collective-permute-start = (bf16[32,512]{1,0:T(8,128)(2,1)S(1)}, bf16[32,512]{1,0:T(8,128)(2,1)S(1)}, u32[]{:S(2)}, u32[]{:S(2)}) collective-permute-start(bf16[32,512]{1,0:T(8,128)(2,1)S(1)} %get-tuple-element.20), channel_id=1, source_target_pairs={{0,1},{1,0},{2,3},{3,2},{4,5},{5,4},{6,7},{7,6},{8,9},{9,8},{10,11... | collective-permute-start | bytes 98312 | tf_op jit(solution)/shard_map/ppermute | solution.py:371
  92.3 0.8 collective-permute-done.other_ref
  93.2 7.8 %all-to-all-done.3 = f32[128,1,128]{2,1,0:T(1,128)S(1)} async-done(((f32[128,1,128]{2,1,0:T(1,128)}), f32[128,1,128]{2,1,0:T(1,128)S(1)}, u32[]{:S(2)}, u32[]{:S(2)}) %all-to-all-start.3) | async-done | bytes 65568 | tf_op jit(solution)/shard_map/all_to_all | solution.py:281
  101.0 1.6 %shard_map.153 = bf16[16,32]{1,0:T(8,128)(2,1)} custom-call(s32[1]{0:T(128)} %bitcast.tp_ref, f32[128,128]{1,0:T(8,128)S(1)} %bitcast.10, bf16[64,512]{1,0:T(8,128)(2,1)} %bitcast.12, bf16[32,512]{1,0:T(8,128)(2,1)S(1)} %collective-permute-done.other_ref), custom_call_target="tpu_custom_call" | custom-call | tf_op jit(solution)/shard_map/pallas_call | solution.py:38
  (2 shorter events, 0.0 us)
Async XLA Ops:
  2.6 30.0 %all-to-all-start = ((bf16[64,16,128]{2,1,0:T(8,128)(2,1)}), bf16[64,16,128]{2,1,0:T(8,128)(2,1)S(1)}, u32[]{:S(2)}, u32[]{:S(2)}) async-start(bf16[64,16,128]{2,1,0:T(8,128)(2,1)} %get-tuple-element.13), calls=%async_computation | async-start | bytes 524288 | tf_op jit(solution)/shard_map/all_to_all | solution.py:281
  61.3 18.2 %all-to-all-start.2 = ((bf16[64,16,128]{2,1,0:T(8,128)(2,1)}), bf16[64,16,128]{2,1,0:T(8,128)(2,1)S(1)}, u32[]{:S(2)}, u32[]{:S(2)}) async-start(bf16[64,16,128]{2,1,0:T(8,128)(2,1)} %get-tuple-element.15), calls=%async_computation.2 | async-start | bytes 524288 | tf_op jit(solution)/shard_map/all_to_all | solution.py:281
  80.7 20.3 %all-to-all-start.3 = ((f32[128,1,128]{2,1,0:T(1,128)}), f32[128,1,128]{2,1,0:T(1,128)S(1)}, u32[]{:S(2)}, u32[]{:S(2)}) async-start(f32[128,1,128]{2,1,0:T(1,128)} %bitcast.7), calls=%async_computation.3 | async-start | bytes 131072 | tf_op jit(solution)/shard_map/all_to_all | solution.py:281
  89.4 3.8 %collective-permute-start = (bf16[32,512]{1,0:T(8,128)(2,1)S(1)}, bf16[32,512]{1,0:T(8,128)(2,1)S(1)}, u32[]{:S(2)}, u32[]{:S(2)}) collective-permute-start(bf16[32,512]{1,0:T(8,128)(2,1)S(1)} %get-tuple-element.20), channel_id=1, source_target_pairs={{0,1},{1,0},{2,3},{3,2},{4,5},{5,4},{6,7},{7,6},{8,9},{9,8},{10,11... | collective-permute-start | bytes 98312 | tf_op jit(solution)/shard_map/ppermute | solution.py:371

commit v3 on v2

--- a/solution.py
+++ b/solution.py
@@ -140,52 +140,65 @@
 
 
 def attend(
-    len_ref, me_ref, got_ref, cache_hbm, rope_hbm, out_ref, q_buf, r_buf, buf, cache_ref, rope_ref, sem
+    len_ref,
+    me_ref,
+    got_ref,
+    cache_hbm,
+    rope_hbm,
+    out_ref,
+    q_buf,
+    r_buf,
+    buf,
+    score_buf,
+    weight_buf,
+    cache_ref,
+    rope_ref,
+    sem,
 ):
-    copies = []
-    for j in range(8):
-        for s in range(2):
-            b = 8 * s + j
-            copies.append(
-                (
-                    pltpu.make_async_copy(cache_hbm.at[b], cache_ref.at[b], sem.at[0, b]),
-                    pltpu.make_async_copy(rope_hbm.at[b], rope_ref.at[b], sem.at[1, b]),
-                )
-            )
-    for pair in copies:
-        for copy in pair:
-            copy.start()
+    copies = [pltpu.make_async_copy(rope_hbm, rope_ref, sem.at[4])] + [
+        pltpu.make_async_copy(
+            cache_hbm.at[4 * g : 4 * g + 4], cache_ref.at[4 * g : 4 * g + 4], sem.at[g]
+        )
+        for g in range(4)
+    ]
+    for copy in copies:
+        copy.start()
     for h in range(8):
         for j in range(8):
             piece = got_ref[8 * h + j].astype(F32)
             q_buf[j, :, h, :] = piece[0:8]
             r_buf[j, h : h + 1, :] = piece[8:9]
-    base = me_ref[0] * 192
-    position = lanes((8, 192)) + base
-    first = lanes((8, 128)) < 64
-    for j in range(8):
-        for s in range(2):
-            b = 8 * s + j
-            q = jnp.concatenate([q_buf[j, 4 * s + c] for c in range(4)], axis=1).astype(BF16)
-            q_rot = r_buf[j][:, 64 * s : 64 * s + 32].astype(BF16)
-            for copy in copies[2 * j + s]:
-                copy.wait()
-            keys = cache_ref[b]
-            scores = lax.dot_general(
-                q, keys, (((1,), (1,)), ((), ())), preferred_element_type=F32
-            ) + jnp.dot(q_rot, rope_ref[b], preferred_element_type=F32)
-            usable = position < len_ref[b]
-            masked = jnp.where(usable, scores * SCALE, NEG)
-            top = jnp.max(masked, axis=1, keepdims=True)
-            weights = jnp.where(usable, jnp.exp(masked - top), 0.0)
-            total = jnp.sum(weights, axis=1, keepdims=True)
-            weighted = jnp.dot(weights.astype(BF16), keys, preferred_element_type=F32)
-            for c in range(4):
-                buf[:, j, 4 * s + c, :] = weighted[:, 128 * c : 128 * c + 128]
-            for i, part in enumerate(split3(top)):
-                buf[:, j, 8 + 4 * s + i, :] = jnp.broadcast_to(part, (8, 128))
-            high, low = split2(total)
-            buf[:, j, 11 + 4 * s, :] = jnp.where(first, high, low)
+    position = lanes((8, 192)) + me_ref[0] * 192
+    first = lanes((128, 128)) < 64
+    copies[0].wait()
+    for b in range(16):
+        s, j = divmod(b, 8)
+        if b % 4 == 0:
+            copies[1 + b // 4].wait()
+        q = jnp.concatenate([q_buf[j, 4 * s + c] for c in range(4)], axis=1).astype(BF16)
+        q_rot = r_buf[j][:, 64 * s : 64 * s + 32].astype(BF16)
+        scores = lax.dot_general(
+            q, cache_ref[b], (((1,), (1,)), ((), ())), preferred_element_type=F32
+        ) + jnp.dot(q_rot, rope_ref[b], preferred_element_type=F32)
+        score_buf[8 * b : 8 * b + 8, :] = jnp.where(position < len_ref[b], scores * SCALE, NEG)
+    masked = score_buf[...]
+    top = jnp.max(masked, axis=1, keepdims=True)
+    weights = jnp.where(masked > 0.5 * NEG, jnp.exp(masked - top), 0.0)
+    weight_buf[...] = weights
+    high, low = split2(jnp.sum(weights, axis=1, keepdims=True))
+    rows = [jnp.broadcast_to(part, (128, 128)) for part in split3(top)]
+    rows.append(jnp.where(first, high, low))
+    for b in range(16):
+        s, j = divmod(b, 8)
+        for i, row in enumerate(rows):
+            buf[:, j, 8 + 4 * s + i, :] = row[8 * b : 8 * b + 8]
+    for b in range(16):
+        s, j = divmod(b, 8)
+        weighted = jnp.dot(
+            weight_buf[8 * b : 8 * b + 8, :].astype(BF16), cache_ref[b], preferred_element_type=F32
+        )
+        for c in range(4):
+            buf[:, j, 4 * s + c, :] = weighted[:, 128 * c : 128 * c + 128]
     out_ref[...] = buf[...].reshape(64, 16, 128).astype(BF16)
 
 
@@ -350,9 +363,11 @@
             pltpu.VMEM((8, 8, 8, 128), F32),
             pltpu.VMEM((8, 8, 128), F32),
             pltpu.VMEM((8, 8, 16, 128), F32),
+            pltpu.VMEM((128, 192), F32),
+            pltpu.VMEM((128, 192), F32),
             pltpu.VMEM((16, 192, 512), BF16),
             pltpu.VMEM((16, 32, 192), BF16),
-            pltpu.SemaphoreType.DMA((2, 16)),
+            pltpu.SemaphoreType.DMA((5,)),
         ],
     )
     latent_new, rope_new, own_latent, half = call(

time: 103 us -> 97.4 us (0.946)
  Pallas kernels: 17.1 us -> 11.4 us
    pallas_call x6, Pallas kernels: 17.1 us -> 11.4 us  [call(): pl.pallas_call(body, out_shape=tuple(shapes), in_specs=[pl.BlockSpec(memo...]
where the time goes in v3:
time: 97.4 us; the launch traced here: 96.8 us
  starting transfers between devices  34.5 us (35%)
  waiting for transfers between devices  29.3 us (30%)
  blocking collectives  17.9 us (18%)
  Pallas kernels  11.4 us (12%)
  other arithmetic  1.58 us (2%)
  local copies, waits for them, and re-layouts  1.49 us (2%)
    all_to_all x3, starting transfers between devices, exchanged(): return lax.all_to_all(value, axes, split_axis=0, concat_axis=0, tiled=True)  31.6 us
    all_to_all x3, waiting for transfers between devices, exchanged(): return lax.all_to_all(value, axes, split_axis=0, concat_axis=0, tiled=True)  28.4 us
    all_to_all x1, blocking collectives, exchanged(): return lax.all_to_all(value, axes, split_axis=0, concat_axis=0, tiled=True)  17.9 us
    pallas_call x6, Pallas kernels, call(): pl.pallas_call(body, out_shape=tuple(shapes), in_specs=[pl.BlockSpec(memo...  11.4 us
    ppermute x1, starting transfers between devices, local(): other = lax.ppermute(half, 'tp', [(0, 1), (1, 0)])  2.91 us
  transfers between devices with their start and end apart: 4, of which 4 were waited for; matrix products, arithmetic and copies ran while one was open for 3% of the time, Pallas kernels for 2%

profile of v3, /device:TPU:1, one launch (start us, length us, event | category | flops | bytes accessed | tf_op | source)
XLA Modules:
  0.0 96.8 jit_solution(959201637537691677)
XLA Ops:
  0.6 2.0 %shard_map.148 = (bf16[64,16,128]{2,1,0:T(8,128)(2,1)}, f32[8,128]{1,0:T(8,128)}) custom-call(bf16[16,64]{1,0:T(8,128)(2,1)} %refs_0_.2, f32[1,64]{1,0:T(1,128)} %bitcast.15, bf16[64,512]{1,0:T(8,128)(2,1)} %refs_2_.1, bf16[64,256]{1,0:T(8,128)(2,1)} %refs_3_.2, bf16[64,512]{1,0:T(8,128)(2,1)} %refs_4_.2, bf16[32,64]{1,0:T(8,128)(2,1)} %bitcast.13, ...), custom_call_target="tpu_custom_call" | custom-call | tf_op jit(solution)/shard_map/pallas_call | solution.py:38
  2.6 17.1 %all-to-all-start = ((bf16[64,16,128]{2,1,0:T(8,128)(2,1)}), bf16[64,16,128]{2,1,0:T(8,128)(2,1)S(1)}, u32[]{:S(2)}, u32[]{:S(2)}) async-start(bf16[64,16,128]{2,1,0:T(8,128)(2,1)} %get-tuple-element.13), calls=%async_computation | async-start | bytes 524288 | tf_op jit(solution)/shard_map/all_to_all | solution.py:294
  19.8 1.3 %fusion.1 = (s32[1]{0:T(128)}, s32[1]{0:T(128)}) fusion(s32[16]{0:T(128)} %refs_0_.3, s32[]{:T(128)S(6)} %select_n.14, s32[]{:T(128)S(6)} %select_n.15), kind=kLoop, calls=%fused_computation.8 | loop fusion | bytes 24 | tf_op jit(solution)/shard_map/dynamic_slice | solution.py:299
  21.1 1.4 %add_convert_fusion = f32[2]{0:T(128)S(1)} fusion(s32[1]{0:T(128)} %get-tuple-element.27, s32[1]{0:T(128)} %get-tuple-element.26), kind=kLoop, calls=%fused_computation.5 | loop fusion | flops 4 | bytes 16 | tf_op jit(solution)/shard_map/convert_element_type | solution.py:299
  22.5 0.1 multiply_cosine_fusion
  22.6 0.1 pad_maximum_fusion
  22.7 0.1 reshape.54
  22.7 0.1 reshape.55
  22.8 9.7 %all-to-all-done.got_ref = bf16[64,16,128]{2,1,0:T(8,128)(2,1)S(1)} async-done(((bf16[64,16,128]{2,1,0:T(8,128)(2,1)}), bf16[64,16,128]{2,1,0:T(8,128)(2,1)S(1)}, u32[]{:S(2)}, u32[]{:S(2)}) %all-to-all-start) | async-done | bytes 262176 | tf_op jit(solution)/shard_map/all_to_all | solution.py:294
  32.6 0.3 shard_map.149
  32.9 17.9 %all_to_all.20.refs_2_.got_ref = bf16[64,16,128]{2,1,0:T(8,128)(2,1)S(1)} all-to-all(bf16[64,16,128]{2,1,0:T(8,128)(2,1)S(1)} %get-tuple-element.14), channel_id=1, replica_groups=mesh['dp'=4,'kv'=64,'tp'=2] {'kv'}, dimensions={0} | all-to-all | bytes 524288 | tf_op jit(solution)/shard_map/all_to_all | solution.py:294
  50.8 4.6 %shard_map.150 = (bf16[64,16,128]{2,1,0:T(8,128)(2,1)}, f32[8,128]{1,0:T(8,128)}) custom-call(s32[16]{0:T(128)} %refs_0_.3, s32[1]{0:T(128)} %bitcast.1.me_ref.refs_1_, bf16[64,16,128]{2,1,0:T(8,128)(2,1)S(1)} %all_to_all.20.refs_2_.got_ref, bf16[16,192,512]{2,1,0:T(8,128)(2,1)} %refs_3_.3, bf16[16,32,192]{2,1,0:T(8,128)(2,1)} %refs_4_.3), custom_call_target="tpu_custom_call" | custom-call | tf_op jit(solution)/shard_map/pallas_call | solution.py:38
  55.5 5.7 %all-to-all-start.2 = ((bf16[64,16,128]{2,1,0:T(8,128)(2,1)}), bf16[64,16,128]{2,1,0:T(8,128)(2,1)S(1)}, u32[]{:S(2)}, u32[]{:S(2)}) async-start(bf16[64,16,128]{2,1,0:T(8,128)(2,1)} %get-tuple-element.15), calls=%async_computation.2 | async-start | bytes 524288 | tf_op jit(solution)/shard_map/all_to_all | solution.py:294
  61.2 1.6 %shard_map.151 = (bf16[16,512]{1,0:T(8,128)(2,1)}, bf16[16,32]{1,0:T(8,128)(2,1)}, f32[8,128]{1,0:T(8,128)S(1)}, bf16[32,512]{1,0:T(8,128)(2,1)S(1)}) custom-call(s32[1]{0:T(128)} %bitcast.1.me_ref.refs_1_, s32[1]{0:T(128)} %bitcast.tp_ref, bf16[64,16,128]{2,1,0:T(8,128)(2,1)S(1)} %all_to_all.20.refs_2_.got_ref, f32[1,512]{1,0:T(1,128)} %bitcast.14, ...), custom_call_target="tpu_custom_call" | custom-call | tf_op jit(solution)/shard_map/pallas_call | solution.py:38
  62.8 10.9 %all-to-all-done.2.refs_0_ = bf16[64,16,128]{2,1,0:T(8,128)(2,1)S(1)} async-done(((bf16[64,16,128]{2,1,0:T(8,128)(2,1)}), bf16[64,16,128]{2,1,0:T(8,128)(2,1)S(1)}, u32[]{:S(2)}, u32[]{:S(2)}) %all-to-all-start.2) | async-done | bytes 262176 | tf_op jit(solution)/shard_map/all_to_all | solution.py:294
  73.7 1.2 %shard_map.152 = (f32[128,128]{1,0:T(8,128)}, f32[8,128]{1,0:T(8,128)}) custom-call(bf16[64,16,128]{2,1,0:T(8,128)(2,1)S(1)} %all-to-all-done.2.refs_0_, bf16[512,128]{1,0:T(8,128)(2,1)S(1)} %get-tuple-element.16.refs_1_, f32[16,128]{1,0:T(8,128)S(1)} %get-tuple-element.17.refs_2_, f32[8,128]{1,0:T(8,128)S(1)} %get-tuple-element.18.refs_3_), custom_call_target="tpu_custom_call" | custom-call | tf_op jit(solution)/shard_map/pallas_call | solution.py:38
  74.9 8.7 %all-to-all-start.3 = ((f32[128,1,128]{2,1,0:T(1,128)}), f32[128,1,128]{2,1,0:T(1,128)S(1)}, u32[]{:S(2)}, u32[]{:S(2)}) async-start(f32[128,1,128]{2,1,0:T(1,128)} %bitcast.7), calls=%async_computation.3 | async-start | bytes 131072 | tf_op jit(solution)/shard_map/all_to_all | solution.py:294
  83.6 2.9 %collective-permute-start = (bf16[32,512]{1,0:T(8,128)(2,1)S(1)}, bf16[32,512]{1,0:T(8,128)(2,1)S(1)}, u32[]{:S(2)}, u32[]{:S(2)}) collective-permute-start(bf16[32,512]{1,0:T(8,128)(2,1)S(1)} %get-tuple-element.20), channel_id=1, source_target_pairs={{0,1},{1,0},{2,3},{3,2},{4,5},{5,4},{6,7},{7,6},{8,9},{9,8},{10,11... | collective-permute-start | bytes 98312 | tf_op jit(solution)/shard_map/ppermute | solution.py:386
  86.6 0.8 collective-permute-done.other_ref
  87.4 7.8 %all-to-all-done.3 = f32[128,1,128]{2,1,0:T(1,128)S(1)} async-done(((f32[128,1,128]{2,1,0:T(1,128)}), f32[128,1,128]{2,1,0:T(1,128)S(1)}, u32[]{:S(2)}, u32[]{:S(2)}) %all-to-all-start.3) | async-done | bytes 65568 | tf_op jit(solution)/shard_map/all_to_all | solution.py:294
  95.2 1.6 %shard_map.153 = bf16[16,32]{1,0:T(8,128)(2,1)} custom-call(s32[1]{0:T(128)} %bitcast.tp_ref, f32[128,128]{1,0:T(8,128)S(1)} %bitcast.10, bf16[64,512]{1,0:T(8,128)(2,1)} %bitcast.12, bf16[32,512]{1,0:T(8,128)(2,1)S(1)} %collective-permute-done.other_ref), custom_call_target="tpu_custom_call" | custom-call | tf_op jit(solution)/shard_map/pallas_call | solution.py:38
  (2 shorter events, 0.0 us)
Async XLA Ops:
  2.6 30.0 %all-to-all-start = ((bf16[64,16,128]{2,1,0:T(8,128)(2,1)}), bf16[64,16,128]{2,1,0:T(8,128)(2,1)S(1)}, u32[]{:S(2)}, u32[]{:S(2)}) async-start(bf16[64,16,128]{2,1,0:T(8,128)(2,1)} %get-tuple-element.13), calls=%async_computation | async-start | bytes 524288 | tf_op jit(solution)/shard_map/all_to_all | solution.py:294
  55.5 18.2 %all-to-all-start.2 = ((bf16[64,16,128]{2,1,0:T(8,128)(2,1)}), bf16[64,16,128]{2,1,0:T(8,128)(2,1)S(1)}, u32[]{:S(2)}, u32[]{:S(2)}) async-start(bf16[64,16,128]{2,1,0:T(8,128)(2,1)} %get-tuple-element.15), calls=%async_computation.2 | async-start | bytes 524288 | tf_op jit(solution)/shard_map/all_to_all | solution.py:294
  74.9 20.3 %all-to-all-start.3 = ((f32[128,1,128]{2,1,0:T(1,128)}), f32[128,1,128]{2,1,0:T(1,128)S(1)}, u32[]{:S(2)}, u32[]{:S(2)}) async-start(f32[128,1,128]{2,1,0:T(1,128)} %bitcast.7), calls=%async_computation.3 | async-start | bytes 131072 | tf_op jit(solution)/shard_map/all_to_all | solution.py:294
  83.6 3.8 %collective-permute-start = (bf16[32,512]{1,0:T(8,128)(2,1)S(1)}, bf16[32,512]{1,0:T(8,128)(2,1)S(1)}, u32[]{:S(2)}, u32[]{:S(2)}) collective-permute-start(bf16[32,512]{1,0:T(8,128)(2,1)S(1)} %get-tuple-element.20), channel_id=1, source_target_pairs={{0,1},{1,0},{2,3},{3,2},{4,5},{5,4},{6,7},{7,6},{8,9},{9,8},{10,11... | collective-permute-start | bytes 98312 | tf_op jit(solution)/shard_map/ppermute | solution.py:386

commit v4 on v3

v4 whole, which is shorter than its diff:
```python
import jax
import jax.numpy as jnp
from jax import lax
from jax.experimental import pallas as pl
from jax.experimental.pallas import tpu as pltpu
from jax.sharding import PartitionSpec as P

D = 4096
NOPE = 64
ROPE = 32
V_DIM = 64
RANK = 512
EPS = 1e-06
THETA = 10000.0
NEG = -1e30
SCALE = (NOPE + ROPE) ** (-0.5)
F32 = jnp.float32
BF16 = jnp.bfloat16
INTERPRET = False


def call(kernel, outs, *args, smem=(), near=(), far=(), results_far=(), scratch=()):
    spaces = [
        pltpu.SMEM if i in smem else pl.ANY if i in far else pltpu.VMEM for i in range(len(args))
    ]
    body = kernel
    shapes = [
        jax.ShapeDtypeStruct(*out) if i in results_far else pltpu.VMEM(*out)
        for i, out in enumerate(outs)
    ]
    if len(outs) == 1 and not results_far:
        shapes.append(pltpu.VMEM((8, 128), F32))

        def body(*refs):
            refs[len(args) + 1][...] = jnp.zeros((8, 128), F32)
            kernel(*refs[: len(args) + 1], *refs[len(args) + 2 :])

    results = pl.pallas_call(
        body,
        out_shape=tuple(shapes),
        in_specs=[pl.BlockSpec(memory_space=space) for space in spaces],
        out_specs=tuple(pl.BlockSpec(memory_space=pltpu.VMEM) for _ in shapes),
        scratch_shapes=list(scratch),
        interpret=INTERPRET,
    )(
        *(
            pltpu.with_memory_space_constraint(a, pltpu.VMEM) if i in near else a
            for i, a in enumerate(args)
        )
    )
    return results[: len(outs)]


def split2(v):
    high = v.astype(BF16).astype(F32)
    return high, v - high


def split3(v):
    high, rest = split2(v)
    mid, low = split2(rest)
    return high, mid, low


def lanes(shape):
    return lax.broadcasted_iota(jnp.int32, shape, len(shape) - 1)


def turn_rows(first_length, second_length):
    lane = lanes((1, 128))
    freq = jnp.full((1, 128), 1.0, F32)
    for i in range(1, ROPE // 2):
        freq = jnp.where(lane % 16 == i, THETA ** (-2.0 * i / ROPE), freq)
    angle = jnp.where(lane < 64, first_length, second_length).astype(F32) * freq
    sine = jnp.sin(angle)
    return jnp.cos(angle), jnp.where(lane % 32 < 16, -sine, sine)


def project(
    me_ref,
    tp_ref,
    len_ref,
    x_ref,
    gain_ref,
    wn_ref,
    wr_ref,
    wl_ref,
    wk_ref,
    uk_ref,
    uv_ref,
    out_ref,
    turn_ref,
    limit_ref,
    buf,
):
    j = me_ref[0] % 8
    cosine, sine = turn_rows(len_ref[j], len_ref[j + 8])
    turn_ref[0:1, :] = cosine
    turn_ref[1:2, :] = sine
    for b in range(16):
        limit_ref[b : b + 1, :] = jnp.full((1, 256), len_ref[b], jnp.int32)
    x = x_ref[...].astype(F32)
    scaled = (x * gain_ref[...]).astype(BF16)
    nope = jnp.dot(scaled, wn_ref[...], preferred_element_type=F32)
    rope = jnp.dot(scaled, wr_ref[...], preferred_element_type=F32)
    latent = jnp.dot(scaled, wl_ref[...], preferred_element_type=F32)
    key = lax.dot_general(
        scaled, wk_ref[...], (((1,), (1,)), ((), ())), preferred_element_type=F32
    )
    squares = jnp.sum(x * x, axis=1, keepdims=True)
    first = lanes((8, 128)) < 64
    square_row = jnp.where(first, squares[:8], squares[8:])
    uk = uk_ref[...].astype(F32)
    uv = uv_ref[...].astype(F32)
    for h in range(8):
        n = slice(64 * h, 64 * h + 64)
        r = slice(32 * h, 32 * h + 32)
        c = slice(128 * (h // 2), 128 * (h // 2) + 128)
        s = slice(8 * (h % 2), 8 * (h % 2) + 8)
        weights = jnp.concatenate([uk[:, n], uv[:, n]], axis=1)
        for t in range(2):
            rows = weights[4 * t : 4 * t + 4]
            buf[t, 32 * h : 32 * h + 32, :] = jnp.concatenate([rows] * 8, axis=0)
        rows = (
            jnp.concatenate([nope[:8, n], nope[8:, n]], axis=1),
            jnp.concatenate([rope[:8, r], key[:8], rope[8:, r], key[8:]], axis=1),
            latent[s, c],
            square_row,
        )
        for i, row in enumerate(rows):
            buf[2, pl.ds(32 * h + i, 8, stride=4), :] = row
    for t in range(3):
        out_ref[:, :, 128 * t : 128 * t + 128] = buf[t].reshape(64, 4, 128).astype(BF16)


def queries(me_ref, got_ref, turn_ref, out_ref, w_ref, own_ref):
    got = got_ref[...].astype(F32)
    weights = jnp.concatenate([got[:, :, 0:128], got[:, :, 128:256]], axis=1)
    weights = weights.reshape(512, 128).astype(BF16)
    w_ref[...] = weights
    total = jnp.sum(got[:, :, 256:384], axis=0)
    nope = total[0:1]
    rope = total[1:2]
    latent = total[2:3]
    inv_rms = lax.rsqrt(total[3:4] / D + EPS)
    lane = lanes((1, 128))
    q_low = (nope * inv_rms).astype(BF16).astype(F32)
    turned = pltpu.roll(q_low, 64, 1)
    row = lax.broadcasted_iota(jnp.int32, (8, 128), 0)
    wide = lanes((8, 128))
    q_wide = jnp.where(row < 4, jnp.broadcast_to(q_low, (8, 128)), jnp.broadcast_to(turned, (8, 128)))
    q_wide = jnp.where(wide < 64, q_wide, 0.0)
    q_latent = jnp.zeros((8, 128), F32)
    for c in range(4):
        left = jnp.where(row % 4 == c, q_wide, 0.0).astype(BF16)
        q_latent = q_latent + lax.dot_general(
            left,
            weights[128 * c : 128 * c + 128],
            (((1,), (1,)), ((), ())),
            preferred_element_type=F32,
        )
    turn = rope * inv_rms
    swapped = jnp.where(lane % 32 < 16, pltpu.roll(turn, 112, 1), pltpu.roll(turn, 16, 1))
    rotated = turn * turn_ref[0:1, :] + swapped * turn_ref[1:2, :]
    other = pltpu.roll(inv_rms, 64, 1)
    odd = (me_ref[0] // 8) % 2 == 1
    latent_rms = jnp.where((lane < 64) == odd, other, inv_rms)
    high, low = split2(latent * latent_rms)
    rest = jnp.concatenate([rotated, high, low, jnp.zeros((1, 128), F32)], axis=0)
    block = jnp.concatenate([q_latent[0:4], q_latent[4:8], rest], axis=1).astype(BF16)
    own_ref[0:8, :] = q_latent.astype(BF16).astype(F32)
    own_ref[8:16, :] = jnp.broadcast_to(rotated.astype(BF16).astype(F32), (8, 128))
    out_ref[...] = jnp.broadcast_to(block[None], (64, 4, 384))


def attend(
    me_ref,
    got_ref,
    limit_ref,
    cache_hbm,
    rope_hbm,
    out_ref,
    q_buf,
    buf,
    score_buf,
    weight_buf,
    cache_ref,
    rope_ref,
    sem,
):
    copies = [pltpu.make_async_copy(rope_hbm, rope_ref, sem.at[4])] + [
        pltpu.make_async_copy(
            cache_hbm.at[4 * g : 4 * g + 4], cache_ref.at[4 * g : 4 * g + 4], sem.at[g]
        )
        for g in range(4)
    ]
    for copy in copies:
        copy.start()
    for h in range(8):
        for t in range(3):
            piece = got_ref[8 * h : 8 * h + 8, :, 128 * t : 128 * t + 128].astype(F32)
            q_buf[t, 40 * h : 40 * h + 32, :] = piece.reshape(32, 128)
    position = lanes((8, 192)) + me_ref[0] * 192
    lane = lanes((128, 128))
    copies[0].wait()
    for b in range(16):
        s, j = divmod(b, 8)
        if b % 8 == 0:
            copies[1 + b // 4].wait()
            copies[2 + b // 4].wait()
        q = [q_buf[s, pl.ds(4 * j + c, 8, stride=40), :] for c in range(4)]
        q = jnp.concatenate(q, axis=1).astype(BF16)
        q_rot = q_buf[2, pl.ds(4 * j, 8, stride=40), :][:, 64 * s : 64 * s + 32].astype(BF16)
        scores = lax.dot_general(
            q, cache_ref[b], (((1,), (1,)), ((), ())), preferred_element_type=F32
        ) + jnp.dot(q_rot, rope_ref[b], preferred_element_type=F32)
        usable = position < limit_ref[b : b + 1, 0:192]
        score_buf[8 * b : 8 * b + 8, :] = jnp.where(usable, scores * SCALE, NEG)
    masked = score_buf[...]
    top = jnp.max(masked, axis=1, keepdims=True)
    weights = jnp.where(masked > 0.5 * NEG, jnp.exp(masked - top), 0.0)
    weight_buf[...] = weights
    sum_high, sum_low = split2(jnp.sum(weights, axis=1, keepdims=True))
    high, mid, low = split3(top)
    row = jnp.where(lane < 64, jnp.where(lane < 32, high, mid), jnp.where(lane < 96, low, sum_high))
    last = jnp.broadcast_to(sum_low, (128, 128))
    for b in range(16):
        s, j = divmod(b, 8)
        buf[2, pl.ds(4 * j + 2 * s, 8, stride=40), :] = row[8 * b : 8 * b + 8]
        buf[2, pl.ds(4 * j + 2 * s + 1, 8, stride=40), :] = last[8 * b : 8 * b + 8]
    for b in range(16):
        s, j = divmod(b, 8)
        weighted = jnp.dot(
            weight_buf[8 * b : 8 * b + 8, :].astype(BF16), cache_ref[b], preferred_element_type=F32
        )
        for c in range(4):
            buf[s, pl.ds(4 * j + c, 8, stride=40), :] = weighted[:, 128 * c : 128 * c + 128]
    for h in range(8):
        for t in range(3):
            piece = buf[t, 40 * h : 40 * h + 32, :].reshape(8, 4, 128).astype(BF16)
            out_ref[8 * h : 8 * h + 8, :, 128 * t : 128 * t + 128] = piece


def new_latents(raw, gain):
    scale = lax.rsqrt(jnp.sum(raw * raw, axis=1, keepdims=True) / RANK + EPS)
    return (raw * scale * gain).astype(BF16)


def new_entries(got_ref, gain_ref, after_ref, latent_ref, rope_ref, buf):
    buf[...] = got_ref[:, :, 256:384].astype(F32).reshape(256, 128)
    turned = buf[pl.ds(0, 8, stride=4), :]
    rope_ref[...] = jnp.concatenate([turned[:, 32:64], turned[:, 96:128]], axis=0).astype(BF16)
    raw = [
        buf[pl.ds(64 * c + 1, 16, stride=4), :] + buf[pl.ds(64 * c + 2, 16, stride=4), :]
        for c in range(4)
    ]
    latent_ref[...] = new_latents(jnp.concatenate(raw, axis=1), gain_ref[...])


def combine(me_ref, got_ref, w_ref, own_q_ref, fresh_ref, gain_ref, out_ref, after_ref, buf):
    buf[...] = got_ref[:, :, 256:384].astype(F32).reshape(256, 128)
    query = own_q_ref[0:8, :]
    turned = own_q_ref[8:9, :]
    lane = lanes((1, 128))
    pair = turned * pltpu.roll(turned, 96, 1)
    j = me_ref[0] % 8
    row = lax.broadcasted_iota(jnp.int32, (8, 128), 0)
    sums = []
    totals = []
    for s in range(2):
        pieces = []
        for c in range(4):
            piece = fresh_ref[16 * c + 8 * s + j].astype(F32)[:, 256:384]
            pieces.append(piece[1:2] + piece[2:3])
        new = new_latents(jnp.concatenate(pieces, axis=1), gain_ref[...]).astype(F32)
        latent = jnp.concatenate([new[:, 128 * c : 128 * c + 128] for c in range(4)], axis=0)
        here = (lane >= 64 * s) & (lane < 64 * s + 32)
        dots = jnp.sum(query[4 * s : 4 * s + 4] * latent, axis=0, keepdims=True)
        own = jnp.sum(dots + jnp.where(here, pair, 0.0), axis=1, keepdims=True) * SCALE
        first = buf[pl.ds(2 * s, 64, stride=4), :]
        second = buf[pl.ds(2 * s + 1, 64, stride=4), :]
        m = first[:, 0:1] + first[:, 32:33] + first[:, 64:65]
        top = jnp.maximum(jnp.max(m, axis=0, keepdims=True), own)
        factor = jnp.exp(m - top)
        own_weight = jnp.exp(own - top)
        total = jnp.sum(factor * (first[:, 96:97] + second[:, 0:1]), axis=0, keepdims=True)
        totals.append(total + own_weight)
        own_low = own_weight.astype(BF16).astype(F32)
        mine = got_ref[:, :, 128 * s : 128 * s + 128].astype(F32)
        sums.append(jnp.sum(mine * factor[:, :, None], axis=0) + own_low * latent)
    weighted_low = jnp.concatenate(sums, axis=0).astype(BF16)
    values = jnp.zeros((8, 128), F32)
    for c in range(4):
        part = jnp.dot(
            weighted_low, w_ref[128 * c : 128 * c + 128, :], preferred_element_type=F32
        )
        values = values + jnp.where(row % 4 == c, part, 0.0)
    front = jnp.sum(values[0:4], axis=0, keepdims=True) / totals[0]
    back = jnp.sum(values[4:8], axis=0, keepdims=True) / totals[1]
    attended = jnp.where(lane < 64, pltpu.roll(front, 64, 1), back).astype(BF16).astype(F32)
    out_ref[...] = jnp.broadcast_to(attended, (128, 128))
    after_ref[...] = jnp.zeros((8, 128), F32)


def half_of(tp_ref, w_ref, after_ref, half_ref):
    half_ref[...] = jnp.where(tp_ref[0] == 0, w_ref[32:64, :], w_ref[0:32, :])


def output(tp_ref, got_ref, w_ref, other_ref, out_ref):
    first = lanes((8, 128)) < 64
    tp = tp_ref[0]
    mixed = jnp.zeros((16, 32), F32)
    for group in range(2):
        pieces = []
        for pair in range(4):
            even = got_ref[pl.ds(32 * pair + group, 8, stride=2), :]
            odd = got_ref[pl.ds(32 * pair + 16 + group, 8, stride=2), :]
            front = jnp.where(first, even, pltpu.roll(odd, 64, 1))
            back = jnp.where(first, pltpu.roll(even, 64, 1), odd)
            pieces.append(jnp.concatenate([front, back], axis=0))
        attended = jnp.concatenate(pieces, axis=1).astype(BF16)
        mine = jnp.where(tp == 0, w_ref[0:32, :], w_ref[32:64, :])
        w = jnp.where(tp == group, mine, other_ref[...])
        part = lax.dot_general(
            attended, w, (((1,), (1,)), ((), ())), preferred_element_type=F32
        )
        mixed = mixed + part.astype(BF16).astype(F32)
    out_ref[...] = mixed.astype(BF16)


def exchanged(value, axes="kv"):
    return lax.all_to_all(value, axes, split_axis=0, concat_axis=0, tiled=True)


def local(
    token_state,
    norm_gain,
    wq_nope,
    wq_rope,
    w_latent,
    w_rope_key,
    kv_gain,
    w_uk,
    w_uv,
    w_out,
    latent_cache,
    rope_cache,
    lengths,
):
    me = lax.axis_index("kv").astype(jnp.int32).reshape(1)
    tp = lax.axis_index("tp").astype(jnp.int32).reshape(1)
    gain = kv_gain.reshape(1, -1)
    w_turned = w_out.T
    block = (64, 4, 384)
    sent, turn, limits = call(
        project,
        [(block, BF16), ((8, 128), F32), ((16, 256), jnp.int32)],
        me,
        tp,
        lengths,
        token_state,
        norm_gain.reshape(1, -1),
        wq_nope,
        wq_rope,
        w_latent,
        w_rope_key.T,
        w_uk,
        w_uv,
        smem=(0, 1, 2),
        scratch=[pltpu.VMEM((3, 256, 128), F32)],
    )
    sent, weights, own_q = call(
        queries,
        [(block, BF16), ((512, 128), BF16), ((16, 128), F32)],
        me,
        exchanged(sent),
        turn,
        smem=(0,),
        near=(1, 2),
    )
    fresh = exchanged(sent)
    (sent,) = call(
        attend,
        [(block, BF16)],
        me,
        fresh,
        limits,
        latent_cache,
        rope_cache,
        smem=(0,),
        near=(1, 2),
        far=(3, 4),
        scratch=[
            pltpu.VMEM((3, 320, 128), F32),
            pltpu.VMEM((3, 320, 128), F32),
            pltpu.VMEM((128, 192), F32),
            pltpu.VMEM((128, 192), F32),
            pltpu.VMEM((16, 192, 512), BF16),
            pltpu.VMEM((16, 32, 192), BF16),
            pltpu.SemaphoreType.DMA((5,)),
        ],
    )
    sent, after = call(
        combine,
        [((128, 128), F32), ((8, 128), F32)],
        me,
        exchanged(sent),
        weights,
        own_q,
        fresh,
        gain,
        smem=(0,),
        near=(1, 2, 3, 4, 5),
        scratch=[pltpu.VMEM((256, 128), F32)],
    )
    arrived = exchanged(sent.reshape(128, 1, 128), ("kv", "tp")).reshape(128, 128)
    (half,) = call(
        half_of,
        [((32, 512), BF16)],
        tp,
        w_turned,
        after,
        smem=(0,),
        near=(1, 2),
    )
    other = lax.ppermute(half, "tp", [(0, 1), (1, 0)])
    latent_new, rope_new = call(
        new_entries,
        [((16, 512), BF16), ((16, 32), BF16)],
        fresh,
        gain,
        after,
        near=(0, 1, 2),
        results_far=(0, 1),
        scratch=[pltpu.VMEM((256, 128), F32)],
    )
    (mixed,) = call(
        output,
        [((16, 32), BF16)],
        tp,
        arrived,
        w_turned,
        other,
        smem=(0,),
        near=(1, 2, 3),
        results_far=(0,),
    )
    return (mixed, latent_new, rope_new)


def solution(mesh):
    in_specs = (
        P("dp", "kv"),
        P("kv"),
        P("kv", "tp"),
        P("kv", "tp"),
        P("kv", None),
        P("kv", None),
        P(),
        P("kv", "tp"),
        P("kv", "tp"),
        P("tp", "kv"),
        P("dp", "kv", None),
        P("dp", None, "kv"),
        P("dp"),
    )
    out_specs = (P("dp", ("kv", "tp")), P("dp", None), P("dp", None))
    return jax.shard_map(local, mesh=mesh, in_specs=in_specs, out_specs=out_specs, check_vma=False)
```

time: 97.4 us -> 90.4 us (0.928)
  blocking collectives: 17.9 us -> 62.8 us
  starting transfers between devices: 34.5 us -> 11 us
  waiting for transfers between devices: 29.3 us -> 7.32 us
  Pallas kernels: 11.4 us -> 8.17 us
  other arithmetic: 1.58 us -> 0 us
  local copies, waits for them, and re-layouts: 1.49 us -> 0.01 us
    all_to_all x1 -> x3, blocking collectives: 17.9 us -> 62.8 us  [exchanged(): return lax.all_to_all(value, axes, split_axis=0, concat_axis=0, tiled=True)]
    all_to_all x3 -> x1, starting transfers between devices: 31.6 us -> 8.09 us  [exchanged(): return lax.all_to_all(value, axes, split_axis=0, concat_axis=0, tiled=True)]
    all_to_all x3 -> x1, waiting for transfers between devices: 28.4 us -> 7.22 us  [exchanged(): return lax.all_to_all(value, axes, split_axis=0, concat_axis=0, tiled=True)]
    pallas_call x6 -> x7, Pallas kernels: 11.4 us -> 8.17 us  [call(): pl.pallas_call(body, out_shape=tuple(shapes), in_specs=[pl.BlockSpec(memo...]
    convert_element_type x1 -> x0, other arithmetic: 1.37 us -> none  [turn_rows(): pair = jnp.stack([lengths[j], lengths[j + 8]]).astype(F32)]
    dynamic_slice x1 -> x0, local copies, waits for them, and re-layouts: 1.32 us -> none  [turn_rows(): pair = jnp.stack([lengths[j], lengths[j + 8]]).astype(F32)]
  transfers between devices with their start and end apart: 4 -> 2, of which waited for: 4 -> 2; matrix products, arithmetic and copies ran while one was open for 3% -> 0% of each run, Pallas kernels for 2% -> 1%
where the time goes in v4:
time: 90.4 us; the launch traced here: 90 us
  blocking collectives  62.8 us (69%)
  starting transfers between devices  11 us (12%)
  Pallas kernels  8.17 us (9%)
  waiting for transfers between devices  7.32 us (8%)
    all_to_all x3, blocking collectives, exchanged(): return lax.all_to_all(value, axes, split_axis=0, concat_axis=0, tiled=True)  62.8 us
    pallas_call x7, Pallas kernels, call(): pl.pallas_call(body, out_shape=tuple(shapes), in_specs=[pl.BlockSpec(memo...  8.17 us
    all_to_all x1, starting transfers between devices, exchanged(): return lax.all_to_all(value, axes, split_axis=0, concat_axis=0, tiled=True)  8.09 us
    all_to_all x1, waiting for transfers between devices, exchanged(): return lax.all_to_all(value, axes, split_axis=0, concat_axis=0, tiled=True)  7.22 us
    ppermute x1, starting transfers between devices, local(): other = lax.ppermute(half, 'tp', [(0, 1), (1, 0)])  2.9 us
  transfers between devices with their start and end apart: 2, of which 2 were waited for; matrix products, arithmetic and copies ran while one was open for 0% of the time, Pallas kernels for 1%

profile of v4, /device:TPU:1, one launch (start us, length us, event | category | flops | bytes accessed | tf_op | source)
XLA Modules:
  0.0 90.0 jit_solution(2369269958546924091)
XLA Ops:
  0.6 0.0 copy-start.1
  0.6 0.0 copy-start
  0.7 1.2 %shard_map.148 = (bf16[64,4,384]{2,1,0:T(4,128)(2,1)S(1)}, f32[8,128]{1,0:T(8,128)S(1)}, s32[16,256]{1,0:T(8,128)S(1)}) custom-call(s32[1]{0:T(128)} %bitcast.1.me_ref.refs_0_, s32[1]{0:T(128)} %bitcast.tp_ref.refs_0_, s32[16]{0:T(128)} %len_ref.1, bf16[16,64]{1,0:T(8,128)(2,1)} %x_ref.1, f32[1,64]{1,0:T(1,128)} %bitcast.16, bf16[64,512]{1,0:T(8,128)(2,1)} %wn_ref.1, ...), custom_call_target="tpu_custom_call" | custom-call | tf_op jit(solution)/shard_map/pallas_call | solution.py:38
  1.9 28.9 %all_to_all.20.got_ref = bf16[64,4,384]{2,1,0:T(4,128)(2,1)S(1)} all-to-all(bf16[64,4,384]{2,1,0:T(4,128)(2,1)S(1)} %get-tuple-element.15), channel_id=1, replica_groups=mesh['dp'=4,'kv'=64,'tp'=2] {'kv'}, dimensions={0} | all-to-all | bytes 393216 | tf_op jit(solution)/shard_map/all_to_all | solution.py:332
  30.9 0.3 shard_map.149
  31.2 17.1 %all_to_all.21.refs_1_.fresh_ref.got_ref = bf16[64,4,384]{2,1,0:T(4,128)(2,1)S(1)} all-to-all(bf16[64,4,384]{2,1,0:T(4,128)(2,1)S(1)} %get-tuple-element.17), channel_id=1, replica_groups=mesh['dp'=4,'kv'=64,'tp'=2] {'kv'}, dimensions={0} | all-to-all | bytes 393216 | tf_op jit(solution)/shard_map/all_to_all | solution.py:332
  48.3 3.2 %shard_map.150 = (bf16[64,4,384]{2,1,0:T(4,128)(2,1)S(1)}, f32[8,128]{1,0:T(8,128)}) custom-call(s32[1]{0:T(128)} %bitcast.1.me_ref.refs_0_, bf16[64,4,384]{2,1,0:T(4,128)(2,1)S(1)} %all_to_all.21.refs_1_.fresh_ref.got_ref, s32[16,256]{1,0:T(8,128)S(1)} %get-tuple-element.18.refs_2_, bf16[16,192,512]{2,1,0:T(8,128)(2,1)} %refs_3_.1, bf16[16,32,192]{2,1,0:T(8,128)(2,1)} %refs_4_.1), custom_call_target="tpu_custom_call" | custom-call | tf_op jit(solution)/shard_map/pallas_call | solution.py:38
  51.5 16.8 %all_to_all.22.got_ref = bf16[64,4,384]{2,1,0:T(4,128)(2,1)S(1)} all-to-all(bf16[64,4,384]{2,1,0:T(4,128)(2,1)S(1)} %get-tuple-element.19), channel_id=1, replica_groups=mesh['dp'=4,'kv'=64,'tp'=2] {'kv'}, dimensions={0} | all-to-all | bytes 393216 | tf_op jit(solution)/shard_map/all_to_all | solution.py:332
  68.3 0.0 copy-done.1
  68.3 1.3 %shard_map.151 = (f32[128,128]{1,0:T(8,128)}, f32[8,128]{1,0:T(8,128)S(1)}) custom-call(s32[1]{0:T(128)} %bitcast.1.me_ref.refs_0_, bf16[64,4,384]{2,1,0:T(4,128)(2,1)S(1)} %all_to_all.22.got_ref, bf16[512,128]{1,0:T(8,128)(2,1)S(1)} %get-tuple-element.20.w_ref, f32[16,128]{1,0:T(8,128)S(1)} %get-tuple-element.21.own_q_ref, ...), custom_call_target="tpu_custom_call" | custom-call | tf_op jit(solution)/shard_map/pallas_call | solution.py:38
  69.6 8.1 %all-to-all-start.3 = ((f32[128,1,128]{2,1,0:T(1,128)}), f32[128,1,128]{2,1,0:T(1,128)S(1)}, u32[]{:S(2)}, u32[]{:S(2)}) async-start(f32[128,1,128]{2,1,0:T(1,128)} %bitcast.6), calls=%async_computation.3 | async-start | bytes 131072 | tf_op jit(solution)/shard_map/all_to_all | solution.py:332
  77.7 0.0 copy-done
  77.7 0.6 shard_map.152
  78.3 2.9 %collective-permute-start = (bf16[32,512]{1,0:T(8,128)(2,1)S(1)}, bf16[32,512]{1,0:T(8,128)(2,1)S(1)}, u32[]{:S(2)}, u32[]{:S(2)}) collective-permute-start(bf16[32,512]{1,0:T(8,128)(2,1)S(1)} %get-tuple-element.24), channel_id=1, source_target_pairs={{0,1},{1,0},{2,3},{3,2},{4,5},{5,4},{6,7},{7,6},{8,9},{9,8},{10,11... | collective-permute-start | bytes 98312 | tf_op jit(solution)/shard_map/ppermute | solution.py:426
  81.2 0.7 shard_map.154
  81.9 0.1 collective-permute-done.other_ref
  82.0 7.2 %all-to-all-done.3 = f32[128,1,128]{2,1,0:T(1,128)S(1)} async-done(((f32[128,1,128]{2,1,0:T(1,128)}), f32[128,1,128]{2,1,0:T(1,128)S(1)}, u32[]{:S(2)}, u32[]{:S(2)}) %all-to-all-start.3) | async-done | bytes 65568 | tf_op jit(solution)/shard_map/all_to_all | solution.py:332
  89.2 0.8 shard_map.153
Async XLA Ops:
  0.6 67.6 %copy-start.1 = (f32[512]{0:T(512)S(1)}, f32[512]{0:T(512)}, u32[]{:S(2)}) copy-start(f32[512]{0:T(512)} %param.19) | copy-start | bytes 6148
  0.6 77.0 %copy-start = (bf16[512,64]{0,1:T(8,128)(2,1)S(1)}, bf16[512,64]{0,1:T(8,128)(2,1)}, u32[]{:S(2)}) copy-start(bf16[512,64]{0,1:T(8,128)(2,1)} %param.22) | copy-start | bytes 196612
  69.6 19.7 %all-to-all-start.3 = ((f32[128,1,128]{2,1,0:T(1,128)}), f32[128,1,128]{2,1,0:T(1,128)S(1)}, u32[]{:S(2)}, u32[]{:S(2)}) async-start(f32[128,1,128]{2,1,0:T(1,128)} %bitcast.6), calls=%async_computation.3 | async-start | bytes 131072 | tf_op jit(solution)/shard_map/all_to_all | solution.py:332
  78.3 3.7 %collective-permute-start = (bf16[32,512]{1,0:T(8,128)(2,1)S(1)}, bf16[32,512]{1,0:T(8,128)(2,1)S(1)}, u32[]{:S(2)}, u32[]{:S(2)}) collective-permute-start(bf16[32,512]{1,0:T(8,128)(2,1)S(1)} %get-tuple-element.24), channel_id=1, source_target_pairs={{0,1},{1,0},{2,3},{3,2},{4,5},{5,4},{6,7},{7,6},{8,9},{9,8},{10,11... | collective-permute-start | bytes 98312 | tf_op jit(solution)/shard_map/ppermute | solution.py:426
